TPU v7x, 32 devices: a whole 2x2x4 slice. The times are simulated.
32 devices in a mesh: sp: 16 (over z, y, x), tp: 2 (over core).
Axes of the slice: x: 2, y: 2, z: 4, core: 2. Of those that a mesh axis runs over, the one named last changes fastest.
Arguments:
- tokens: bfloat16 [4096, 2048], P('sp'), as said below
- in_gain: float32 [2048], replicated, may hold values from 0.1 to 1.9
- w_query: bfloat16 [2048, 1024], P(None, 'tp'), as said below
- w_key: bfloat16 [2048, 1024], P(None, 'tp'), may hold values from -0.125 to 0.125
- w_value: bfloat16 [2048, 1024], P(None, 'tp'), may hold values from -0.125 to 0.125
- lam: float32 [8], P('tp'), may hold values from 0.3 to 0.8
- sub_gain: float32 [128], replicated, may hold values from 0.1 to 1.9
- w_out: bfloat16 [1024, 2048], P('tp'), may hold values from -0.1875 to 0.1875
Outputs:
- mixed: bfloat16 [4096, 2048], P('sp')
Inputs may be any that keep to these rules, and one draw needn't show every extreme that they name: tokens: normal entries plus, for each block of 64 tokens, a factor times one direction common to all tokens. w_query: independent normal entries.
All inputs are finite; a program needn't handle non-finite values.
Results may differ from a plain program's by a relative error of at most 0.025.
The roundings to bfloat16 on the way count: a program that leaves them out, or rounds other values in their place, can miss the bound.
Values may be sent and summed in bfloat16 or wider, within the bound.
No kernel may reach another device: no remote copies, remote signals or barrier semaphores. Data moves between devices by JAX's collectives and lax.ppermute only.
A program may use at most 64 MiB of HBM per device.

v0:
```python
import jax
import jax.numpy as jnp
from jax import lax
from jax.sharding import PartitionSpec as P

KD = 64
VD = 128


def rotate(vectors, position):
    half = vectors.shape[-1] // 2
    freq = 500000.0 ** (-jnp.arange(0, 2 * half, 2, dtype=jnp.float32) / (2 * half))
    angle = position.astype(jnp.float32)[:, None] * freq[None, :]
    cosine = jnp.cos(angle)[:, None, :]
    sine = jnp.sin(angle)[:, None, :]
    first = vectors[..., :half]
    second = vectors[..., half:]
    return jnp.concatenate(
        [first * cosine - second * sine, second * cosine + first * sine], axis=-1
    )


def shards(tokens, in_gain, w_query, w_key, w_value, lam, sub_gain, w_out):
    span = tokens.shape[0]
    local_heads = lam.shape[0]
    xfloat = tokens.astype(jnp.float32)
    normed = (
        xfloat * lax.rsqrt(jnp.mean(xfloat * xfloat, axis=-1, keepdims=True) + 1e-06) * in_gain
    ).astype(jnp.bfloat16)
    weights_all = jnp.concatenate([w_query, w_key, w_value], axis=1)
    projected = jnp.dot(normed, weights_all, preferred_element_type=jnp.float32)
    qcols = local_heads * 2 * KD
    position = lax.axis_index("sp") * span + jnp.arange(span, dtype=jnp.int32)
    queries = rotate(projected[:, :qcols].reshape(span, 2 * local_heads, KD), position).astype(
        jnp.bfloat16
    )
    queries = queries.reshape(span, local_heads, 2, KD)
    keys = rotate(
        projected[:, qcols : 2 * qcols].reshape(span, 2 * local_heads, KD), position
    ).astype(jnp.bfloat16)
    keys = keys.reshape(span, qcols)
    values = projected[:, 2 * qcols :].astype(jnp.bfloat16)
    scale = KD ** (-0.5)

    def update(carry, key_piece, value_piece):
        top, mass, accum = carry
        count = key_piece.shape[0]
        key_four = key_piece.reshape(count, local_heads, 2, KD)
        value_three = value_piece.reshape(count, local_heads, VD)
        scores = (
            jnp.einsum("qhcd,khcd->hcqk", queries, key_four, preferred_element_type=jnp.float32)
            * scale
        )
        new_top = jnp.maximum(top, jnp.max(scores, axis=-1))
        factor = jnp.exp(top - new_top)
        expo = jnp.exp(scores - new_top[..., None])
        mass = mass * factor + jnp.sum(expo, axis=-1)
        weights = expo.astype(jnp.bfloat16)
        accum = accum * factor[..., None] + jnp.einsum(
            "hcqk,khe->hcqe", weights, value_three, preferred_element_type=jnp.float32
        )
        return (new_top, mass, accum)

    start_carry = (
        jnp.full((local_heads, 2, span), -1e30, jnp.float32),
        jnp.zeros((local_heads, 2, span), jnp.float32),
        jnp.zeros((local_heads, 2, span, VD), jnp.float32),
    )
    carry = start_carry
    key_piece = lax.all_gather(keys, "sp", axis=0, tiled=True)
    value_piece = lax.all_gather(values, "sp", axis=0, tiled=True)
    count = key_piece.shape[0]

    def step_block(inner, items):
        return (update(inner, items[0], items[1]), None)

    blocks = (
        key_piece.reshape(count // 512, 512, key_piece.shape[1]),
        value_piece.reshape(count // 512, 512, value_piece.shape[1]),
    )
    carry, unused = lax.scan(step_block, carry, blocks)
    top, mass, accum = carry
    read = accum / mass[..., None]
    diff = read[:, 0] - lam[:, None, None] * read[:, 1]
    normal = diff * lax.rsqrt(jnp.mean(diff * diff, axis=-1, keepdims=True) + 1e-05) * sub_gain
    attended = jnp.transpose(normal, (1, 0, 2)).reshape(span, local_heads * VD).astype(jnp.bfloat16)
    share = lax.psum_scatter(
        jnp.dot(attended, w_out, preferred_element_type=jnp.float32).astype(jnp.bfloat16),
        "tp",
        scatter_dimension=0,
        tiled=True,
    )
    result = lax.all_gather(share, "tp", axis=0, tiled=True)
    return result


def solution(mesh):
    in_specs = (
        P("sp", None),
        P(),
        P(None, "tp"),
        P(None, "tp"),
        P(None, "tp"),
        P("tp"),
        P(),
        P("tp", None),
    )
    out_specs = P("sp", None)
    return jax.shard_map(shards, mesh=mesh, in_specs=in_specs, out_specs=out_specs, check_vma=False)
```

profile of v0, /device:TPU:0, one launch (start us, length us, event | category | flops | bytes accessed | tf_op | source)
XLA Modules:
  0.0 281.3 jit_solution(3731221670889648921)
XLA Ops:
  6.6 1.7 fusion.19
  8.2 5.0 %fusion.13 = f32[256,1536]{1,0:T(8,128)S(1)} fusion(bf16[2048,512]{1,0:T(8,128)(2,1)} %param.14, bf16[2048,512]{1,0:T(8,128)(2,1)} %param.13, bf16[2048,512]{1,0:T(8,128)(2,1)} %param.12, bf16[256,2048]{1,0:T(8,128)(2,1)} %param.10, f32[2048]{0:T(1024)} %param.11, f32[256]{0:T(256)S(1)} %add_rsqrt_fusion.1), kind=kOutput, calls=%fused_computation.18 | convolution fusion | flops 1631584256 | bytes 8922112 | tf_op jit(solution)/shard_map/dot_general | solution.py:31
  17.2 1.8 slice.71
  19.2 87.7 %all-gather.4.cloned.1.call-done = bf16[4096,512]{0,1:T(8,128)(2,1)} async-done(((bf16[256,512]{0,1:T(8,128)(2,1)}), bf16[4096,512]{0,1:T(8,128)(2,1)}) %all-gather.4.cloned.1.call-update) | async-done | bytes 4194320 | tf_op jit(solution)/shard_map/all_gather | solution.py:70
  106.8 6.5 %copy.16 = bf16[4096,512]{1,0:T(8,128)(2,1)} copy(bf16[4096,512]{0,1:T(8,128)(2,1)} %all-gather.4.cloned.1.call-done) | data formatting | bytes 8388608 | tf_op jit(solution)/shard_map/all_gather | solution.py:70
  113.3 70.1 %all-gather.6.cloned.1.call-done = bf16[4096,512]{1,0:T(8,128)(2,1)} async-done(((bf16[256,512]{1,0:T(8,128)(2,1)}), bf16[4096,512]{1,0:T(8,128)(2,1)}) %all-gather.6.cloned.1.call-update) | async-done | bytes 4194320 | tf_op jit(solution)/shard_map/all_gather | solution.py:71
  183.4 66.4 %while.15 = (s32[]{:T(128)}, f32[4,2,256]{2,1,0:T(2,128)S(1)}, f32[4,2,256]{2,1,0:T(2,128)S(1)}, f32[4,2,256,128]{3,2,1,0:T(8,128)}, bf16[8,512,512]{2,1,0:T(8,1...) while((s32[]{:T(128)}, f32[4,2,256]{2,1,0:T(2,128)S(1)}, ...), condition=%wide.region_4.5_spmd.clone, body=%wide.region_1.4_spmd.clone.sunk | while | flops 411838464 | bytes 30802120 | solution.py:81
  183.4 2.1 constant_dynamic-slice_fusion.3
  185.5 1.3 copy.30
  189.4 1.4 fusion.49
  191.7 2.1 constant_dynamic-slice_fusion.3
  193.8 1.3 copy.30
  197.7 1.4 fusion.49
  200.0 2.1 constant_dynamic-slice_fusion.3
  206.0 1.4 fusion.49
  208.3 2.1 constant_dynamic-slice_fusion.3
  214.3 1.4 fusion.49
  216.6 2.1 constant_dynamic-slice_fusion.3
  222.6 1.4 fusion.49
  224.9 2.1 constant_dynamic-slice_fusion.3
  230.9 1.4 fusion.49
  233.3 2.1 constant_dynamic-slice_fusion.3
  235.3 1.3 copy.30
  239.2 1.4 fusion.49
  241.6 2.1 constant_dynamic-slice_fusion.3
  243.6 1.3 copy.30
  247.5 1.4 fusion.49
  249.9 1.6 copy.21
  251.9 1.7 convolution_convert_fusion
  253.7 7.1 %reduce-scatter.2.cloned.1.call-done = bf16[128,2048]{1,0:T(8,128)(2,1)} async-done(((bf16[256,2048]{1,0:T(8,128)(2,1)}), bf16[128,2048]{1,0:T(8,128)(2,1)}) %reduce-scatter.2.cloned.1.call-update) | async-done | bytes 524304 | tf_op jit(solution)/shard_map/reduce_scatter | solution.py:87
  260.8 11.7 %all-gather.8.cloned.1.call-done = bf16[256,2048]{1,0:T(8,128)(2,1)} async-done(((bf16[128,2048]{1,0:T(8,128)(2,1)}), bf16[256,2048]{1,0:T(8,128)(2,1)}) %all-gather.8.cloned.1.call-update) | async-done | bytes 1048592 | tf_op jit(solution)/shard_map/all_gather | solution.py:93
  272.5 2.3 copy.45
  (134 shorter events, 37.6 us)
Async XLA Ops:
  6.5 245.4 %copy-start = (bf16[512,2048]{1,0:T(8,128)(2,1)S(1)}, bf16[512,2048]{1,0:T(8,128)(2,1)}, u32[]{:S(2)}) copy-start(bf16[512,2048]{1,0:T(8,128)(2,1)} %param.17) | copy-start | bytes 6291460
  6.5 100.3 %all-gather.4.cloned.1.call-start = ((), (), s32[]{:S(2)}) async-start(), calls=%async_computation.1 | async-start | bytes 4456448 | tf_op jit(solution)/shard_map/all_gather | solution.py:70
  13.3 1.4 copy-start.4
  17.2 166.2 %all-gather.6.cloned.1.call-start = ((), (), s32[]{:S(2)}) async-start(), calls=%async_computation.2 | async-start | bytes 4456448 | tf_op jit(solution)/shard_map/all_gather | solution.py:71
  19.1 241.7 %reduce-scatter.2.cloned.1.call-start = ((), (), s32[]{:S(2)}) async-start(), calls=%async_computation.3 | async-start | bytes 1572864 | tf_op jit(solution)/shard_map/reduce_scatter | solution.py:87
  187.8 1.5 copy-start.1
  187.8 1.5 copy-start.2
  190.8 1.0 copy-start.3
  196.1 1.5 copy-start.1
  196.1 1.5 copy-start.2
  199.1 1.0 copy-start.3
  204.4 1.5 copy-start.1
  204.4 1.5 copy-start.2
  207.4 1.0 copy-start.3
  212.7 1.5 copy-start.1
  212.7 1.5 copy-start.2
  215.7 1.0 copy-start.3
  221.0 1.5 copy-start.1
  221.0 1.5 copy-start.2
  224.0 1.0 copy-start.3
  229.3 1.5 copy-start.1
  229.3 1.5 copy-start.2
  232.3 1.0 copy-start.3
  237.6 1.5 copy-start.1
  237.6 1.5 copy-start.2
  240.6 1.0 copy-start.3
  245.9 1.5 copy-start.1
  245.9 1.5 copy-start.2
  248.9 1.0 copy-start.3
  249.9 1.7 copy-start.5
  249.9 1.9 copy-start.6
  253.6 18.8 %all-gather.8.cloned.1.call-start = ((), (), s32[]{:S(2)}) async-start(), calls=%async_computation.4 | async-start | bytes 1572864 | tf_op jit(solution)/shard_map/all_gather | solution.py:93
Sparse Core Ops, SparseCore 0:
  17.3 89.4 all-gather.3
  109.6 73.7 all-gather.5
  253.8 6.9 reduce-scatter.1
  262.2 10.2 all-gather.7
where the time goes:
time: 282 us; the launch traced here: 281 us
  waiting for transfers between devices  177 us (63%)
  local copies, waits for them, and re-layouts  57.7 us (20%)
  matrix products  24.1 us (9%)
  between operations  13.3 us (5%)
  other arithmetic  9.1 us (3%)
    all_gather x1, waiting for transfers between devices, shards(): key_piece = lax.all_gather(keys, 'sp', axis=0, tiled=True)  87.7 us
    all_gather x1, waiting for transfers between devices, shards(): value_piece = lax.all_gather(values, 'sp', axis=0, tiled=True)  70.1 us
    dynamic_slice x24, local copies, waits for them, and re-layouts, shards(): carry, unused = lax.scan(step_block, carry, blocks)  35 us
    all_gather x1, waiting for transfers between devices, shards(): result = lax.all_gather(share, 'tp', axis=0, tiled=True)  11.7 us
    dot_general x8, matrix products, update(): jnp.einsum('hcqk,khe->hcqe', weights, value_three, preferred_element_type...  11.1 us
    while x56, local copies, waits for them, and re-layouts  7.71 us
    reduce_scatter x1, waiting for transfers between devices, shards(): lax.psum_scatter(jnp.dot(attended, w_out, preferred_element_type=jnp.floa...  7.07 us
    all_gather x1, local copies, waits for them, and re-layouts, shards(): key_piece = lax.all_gather(keys, 'sp', axis=0, tiled=True)  6.49 us
  transfers between devices with their start and end apart: 4, of which 4 were waited for; matrix products, arithmetic and copies ran while one was open for 3% of the time, Pallas kernels for 0%

commit v1 on v0

v1 whole, which is shorter than its diff:
```python
import functools

import jax
import jax.numpy as jnp
from jax import lax
from jax.experimental import pallas as pl
from jax.experimental.pallas import tpu as pltpu
from jax.sharding import PartitionSpec as P

KD = 64
VD = 128
LOG2E = 1.4426950408889634
F32 = jnp.float32
BF16 = jnp.bfloat16
VMEM_LIMIT = 58 * 1024 * 1024


def whole_spec():
    return pl.BlockSpec(memory_space=pltpu.VMEM)


def smem_spec():
    return pl.BlockSpec(memory_space=pltpu.SMEM)


def halves(block):
    return jnp.concatenate(
        [block[:, at : at + 128] for at in range(0, block.shape[1], 128)], axis=0
    )


def unhalve(block):
    return jnp.concatenate(
        [block[at : at + 128, :] for at in range(0, block.shape[0], 128)], axis=1
    )


def project_body(zi, x, gain, cosine, sine, wq, wk, wv, *rest):
    outs, normed = rest[:-1], rest[-1]
    at = pl.program_id(0)
    span = x.shape[0]

    @pl.when(at == 0)
    def _():
        xf = x[...].astype(F32)
        inv = lax.rsqrt(jnp.mean(xf * xf, axis=-1, keepdims=True) + 1e-06)
        normed[...] = (xf * inv * gain[...]).astype(BF16)

    n = normed[...]
    qk = jnp.dot(n, jnp.concatenate([wq[...], wk[...]], axis=1), preferred_element_type=F32)
    v = jnp.dot(n, wv[...], preferred_element_type=F32)
    low = lax.broadcasted_iota(jnp.int32, (span, 2 * KD), 1) % KD < KD // 2

    def rotate(a):
        other = jnp.where(low, pltpu.roll(a, 2 * KD - KD // 2, 1), pltpu.roll(a, KD // 2, 1))
        return a * cosine[...] + other * sine[...]

    k = rotate(qk[:, 2 * KD :]).astype(BF16)
    vt = halves(v.T.astype(BF16))
    qt = halves(rotate(qk[:, : 2 * KD]).T.astype(BF16))
    for index, out in enumerate(outs):

        @pl.when(at == index)
        def _():
            out[0:span] = k
            out[span : 2 * span] = vt
            out[2 * span : 3 * span] = qt


def project(zi, tokens, in_gain, cosine, sine, w_query, w_key, w_value, heads):
    span, width = tokens.shape
    fixed = lambda i, z: (0, 0)
    weight = pl.BlockSpec((width, VD), lambda i, z: (0, jnp.bitwise_xor(z[0], i)))
    return pl.pallas_call(
        project_body,
        grid_spec=pltpu.PrefetchScalarGridSpec(
            num_scalar_prefetch=1,
            grid=(heads,),
            in_specs=[
                pl.BlockSpec((span, width), fixed),
                pl.BlockSpec((1, width), fixed),
                pl.BlockSpec((span, 2 * KD), fixed),
                pl.BlockSpec((span, 2 * KD), fixed),
                weight,
                weight,
                weight,
            ],
            out_specs=[pl.BlockSpec((3 * span, VD), fixed)] * heads,
            scratch_shapes=[pltpu.VMEM((span, width), BF16)],
        ),
        out_shape=[jax.ShapeDtypeStruct((3 * span, VD), BF16)] * heads,
        compiler_params=pltpu.CompilerParams(
            dimension_semantics=("arbitrary",), vmem_limit_bytes=VMEM_LIMIT
        ),
        name="project",
    )(zi, tokens, in_gain[None, :], cosine, sine, w_query, w_key, w_value)


def attend_body(*refs, nq, span, counts, first, last):
    refs = list(refs)
    take = lambda n: [refs.pop(0) for _ in range(n)]
    qs = take(nq)
    kvs = take(len(counts))
    carry_in = [] if first else take(3)
    extra = take(2) if last else []
    outs = take(nq) if last else take(3)
    kscr, vscr, qscr, sscr = take(4)
    blocks = 2 * nq
    total = sum(counts)
    pair = vscr.shape[2] // span
    step = pair * span
    steps = total // pair

    at = 0
    for kv, count in zip(kvs, counts):
        for j in range(count):
            kscr[at * span : (at + 1) * span] = kv[j, 0:span]
            vscr[at // pair, :, (at % pair) * span : (at % pair + 1) * span] = unhalve(
                kv[j, span : 2 * span]
            )
            at += 1
    row = lax.broadcasted_iota(jnp.int32, (2 * KD, span), 0) < KD
    for d in range(nq):
        q = unhalve(qs[d][2 * span : 3 * span]).astype(F32) * (KD**-0.5 * LOG2E)
        high = q.astype(BF16)
        rest = (q - high.astype(F32)).astype(BF16)
        zero = jnp.zeros_like(high)
        for c in range(2):
            mask = row if c == 0 else jnp.logical_not(row)
            qscr[2 * d + c, 0 : 2 * KD] = jnp.where(mask, high, zero)
            qscr[2 * d + c, 2 * KD : 4 * KD] = jnp.where(mask, rest, zero)

    def groups(a):
        return a.reshape(a.shape[0] // 8, 8, a.shape[1])

    def score(b, slot, i, m8):
        k = kscr[pl.ds(pl.multiple_of(i * step, step), step), :]
        s = jnp.dot(jnp.concatenate([k, k], axis=1), qscr[b], preferred_element_type=F32)
        sscr[slot, pl.ds(pl.multiple_of(i * step, step), step), :] = s
        return jnp.maximum(m8, jnp.max(groups(s), axis=0))

    def spread(m8):
        return jnp.broadcast_to(jnp.max(m8, axis=0, keepdims=True), m8.shape)

    low = jnp.full((8, span), -1e30, F32)
    zero8 = jnp.zeros((8, span), F32)
    state = []
    m8 = lax.fori_loop(0, steps, lambda i, m: score(0, 0, i, m), low if first else carry_in[0][0])
    for b in range(blocks):
        m = spread(m8)
        if first:
            mass0 = zero8
            acc0 = jnp.zeros((VD, span), F32)
        else:
            fix = jnp.exp2(carry_in[0][b] - m)
            mass0 = carry_in[1][b] * fix
            acc0 = (groups(carry_in[2][b]) * fix[None]).reshape(VD, span)

        def body(i, carry, b=b, m=m):
            next8, mass, acc = carry
            s = sscr[b % 2, pl.ds(pl.multiple_of(i * step, step), step), :]
            p = jnp.exp2(groups(s) - m[None])
            mass = mass + jnp.sum(p, axis=0)
            acc = acc + jnp.dot(
                vscr[i], p.reshape(step, span).astype(BF16), preferred_element_type=F32
            )
            if b + 1 < blocks:
                next8 = score(b + 1, (b + 1) % 2, i, next8)
            return next8, mass, acc

        next0 = low if first or b + 1 == blocks else carry_in[0][b + 1]
        m8, mass, acc = lax.fori_loop(0, steps, body, (next0, mass0, acc0))
        if not last:
            outs[0][b] = m
            outs[1][b] = mass
            outs[2][b] = acc
            continue
        read = acc / jnp.sum(mass, axis=0, keepdims=True)
        if b % 2 == 0:
            state = read
        else:
            lam, gain = extra
            diff = state - lam[0] * read
            inv = lax.rsqrt(jnp.mean(diff * diff, axis=0, keepdims=True) + 1e-05)
            outs[b // 2][...] = (diff * inv * gain[...]).T.astype(BF16)


def attend(qs, kvs, carry, finish, span):
    nq = len(qs)
    counts = tuple(kv.shape[0] for kv in kvs)
    total = sum(counts)
    pair = next(n for n in (4, 2, 1) if total % n == 0)
    blocks = 2 * nq
    first, last = carry is None, finish is not None
    args = [*qs, *kvs, *(carry or ()), *(finish or ())]
    specs = [whole_spec() for _ in args]
    if last:
        specs[-2] = smem_spec()
        out_shape = [jax.ShapeDtypeStruct((span, VD), BF16)] * nq
    else:
        out_shape = [
            jax.ShapeDtypeStruct((blocks, 8, span), F32),
            jax.ShapeDtypeStruct((blocks, 8, span), F32),
            jax.ShapeDtypeStruct((blocks, VD, span), F32),
        ]
    return pl.pallas_call(
        functools.partial(
            attend_body, nq=nq, span=span, counts=counts, first=first, last=last
        ),
        in_specs=specs,
        out_specs=[whole_spec() for _ in out_shape],
        out_shape=out_shape,
        scratch_shapes=[
            pltpu.VMEM((total * span, VD), BF16),
            pltpu.VMEM((total // pair, VD, pair * span), BF16),
            pltpu.VMEM((blocks, 4 * KD, span), BF16),
            pltpu.VMEM((2, total * span, span), F32),
        ],
        compiler_params=pltpu.CompilerParams(vmem_limit_bytes=VMEM_LIMIT),
        name="attend",
    )(*args)


def output_body(zi, *refs):
    out, scr = refs[-2:]
    weights = refs[-4:-2]
    pieces = refs[:-4]
    heads = len(pieces) // 2

    @pl.when(pl.program_id(0) == 0)
    def _():
        for index, piece in enumerate(pieces):
            side, d = divmod(index, heads)
            head = jnp.bitwise_xor(zi[0], d)
            scr[side, :, pl.ds(pl.multiple_of(head * VD, VD), VD)] = piece[...]

    total = jnp.dot(scr[0], weights[0][...], preferred_element_type=F32)
    total = total + jnp.dot(scr[1], weights[1][...], preferred_element_type=F32)
    out[...] = total.astype(BF16)


def output(zi, own, other, w_own, w_other):
    span = own[0].shape[0]
    rows, width = w_own.shape
    tile = 512
    fixed = lambda i, z: (0, 0)
    piece = pl.BlockSpec((span, VD), fixed)
    weight = pl.BlockSpec((rows, tile), lambda i, z: (0, i))
    return pl.pallas_call(
        output_body,
        grid_spec=pltpu.PrefetchScalarGridSpec(
            num_scalar_prefetch=1,
            grid=(width // tile,),
            in_specs=[piece] * (2 * len(own)) + [weight, weight],
            out_specs=pl.BlockSpec((span, tile), lambda i, z: (0, i)),
            scratch_shapes=[pltpu.VMEM((2, span, rows), BF16)],
        ),
        out_shape=jax.ShapeDtypeStruct((span, width), BF16),
        compiler_params=pltpu.CompilerParams(
            dimension_semantics=("arbitrary",), vmem_limit_bytes=VMEM_LIMIT
        ),
        name="output",
    )(zi, *own, *other, w_own, w_other)


def shards(tokens, in_gain, w_query, w_key, w_value, lam, sub_gain, w_out, *, size, tp):
    span = tokens.shape[0]
    heads = lam.shape[0]
    split = heads if heads & (heads - 1) == 0 and size % heads == 0 else 1
    rest = size // split
    where = lax.axis_index("sp")
    zi = where // rest

    def swap_far(a, d):
        return lax.ppermute(
            a, "sp", [(i, ((i // rest) ^ d) * rest + i % rest) for i in range(size)]
        )

    def swap_near(a, d):
        return lax.ppermute(a, "sp", [(i, i ^ d) for i in range(size)])

    position = (where * span + jnp.arange(span, dtype=jnp.int32)).astype(F32)
    freq = 500000.0 ** (-jnp.arange(0, KD, 2, dtype=F32) / KD)
    angle = position[:, None] * freq[None, :]
    cosine, sine = jnp.cos(angle), jnp.sin(angle)
    cosine = jnp.concatenate([cosine] * 4, axis=1)
    sine = jnp.concatenate([-sine, sine, -sine, sine], axis=1)
    index = zi.astype(jnp.int32)[None] if split == heads else jnp.zeros((1,), jnp.int32)
    parts = project(index, tokens, in_gain, cosine, sine, w_query, w_key, w_value, heads)
    gain = sub_gain[:, None]

    if split == heads:
        mine = [parts[0]] + [None] * (heads - 1)
        for d in sorted(range(1, heads), key=lambda n: -(n ^ 1)):
            mine[d] = swap_far(parts[d], d)
        kv = jnp.stack([a[: 2 * span] for a in mine])
        if rest == 4:
            half = heads // 2 if heads > 1 else 1
            left, right = swap_near(kv, 1), swap_near(kv, 2)
            cross = [swap_near(left[:half], 2)]
            if heads > 1:
                cross.append(swap_near(right[half:], 1))
            pieces = [[kv, left, right, *cross]]
        else:
            groups = [[g * rest + r for r in range(rest)] for g in range(split)]
            kw = {} if split == 1 else {"axis_index_groups": groups}
            every = lax.all_gather(kv, "sp", axis=0, tiled=True, **kw)
            pieces = [[every[at : at + 16]] for at in range(0, every.shape[0], 16)]
        lam_mine = lax.dynamic_slice_in_dim(lam, index[0], 1)
        carry = None
        for at, piece in enumerate(pieces):
            finish = (lam_mine, gain) if at + 1 == len(pieces) else None
            carry = attend(mine, piece, carry, finish, span)
        own = [carry[0]] + [swap_far(carry[d], d) for d in range(1, heads)]
    else:
        own = []
        for h in range(heads):
            every = lax.all_gather(parts[h][None, : 2 * span], "sp", axis=0, tiled=True)
            carry = None
            for at in range(0, size, 16):
                finish = (lam[h : h + 1], gain) if at + 16 >= size else None
                carry = attend([parts[h]], [every[at : at + 16]], carry, finish, span)
            own.append(carry[0])

    if tp == 2:
        flip = [(0, 1), (1, 0)]
        w_other = lax.ppermute(w_out, "tp", flip)
        other = [lax.ppermute(a, "tp", flip) for a in own]
        return output(index, own, other, w_out, w_other)
    attended = jnp.concatenate(own, axis=1)
    if tp > 1:
        attended = lax.all_gather(attended, "tp", axis=1, tiled=True)
        w_out = lax.all_gather(w_out, "tp", axis=0, tiled=True)
    return jnp.dot(attended, w_out, preferred_element_type=F32).astype(BF16)


def solution(mesh):
    in_specs = (
        P("sp", None),
        P(),
        P(None, "tp"),
        P(None, "tp"),
        P(None, "tp"),
        P("tp"),
        P(),
        P("tp", None),
    )
    body = functools.partial(shards, size=mesh.shape["sp"], tp=mesh.shape["tp"])
    return jax.shard_map(
        body, mesh=mesh, in_specs=in_specs, out_specs=P("sp", None), check_vma=False
    )
```

time: 282 us -> 92.6 us (0.33)
  waiting for transfers between devices: 177 us -> 32.8 us
  local copies, waits for them, and re-layouts: 57.7 us -> 7.26 us
  Pallas kernels: 0 us -> 31 us
  matrix products: 24.1 us -> 0 us
  starting transfers between devices: 0.13 us -> 19.5 us
  between operations: 13.3 us -> 0.19 us
  other arithmetic: 9.1 us -> 1.6 us
    all_gather x3 -> x0, waiting for transfers between devices: 169 us -> none  [the longest x1 87.7 us: shards(): key_piece = lax.all_gather(keys, 'sp', axis=0, tiled=True)]
    dynamic_slice x24 -> x1, local copies, waits for them, and re-layouts: 35 us -> 0.6 us  [shards(): lam_mine = lax.dynamic_slice_in_dim(lam, index[0], 1)]
    ppermute x0 -> x15, waiting for transfers between devices: none -> 32.8 us  [the longest x6 18.3 us: swap_far(): lax.ppermute(a, 'sp', [(i, (i // rest ^ d) * rest + i % rest) for i in ra...]
    pallas_call x0 -> x3, Pallas kernels: none -> 31 us  [the longest x1 18.2 us: attend(): pl.pallas_call(functools.partial(attend_body, nq=nq, span=span, counts=co...]
    dot_general x18 -> x0, matrix products: 24.1 us -> none  [the longest x8 11.1 us: update(): jnp.einsum('hcqk,khe->hcqe', weights, value_three, preferred_element_type...]
    ppermute x0 -> x15, starting transfers between devices: none -> 19.5 us  [the longest x6 12.4 us: swap_far(): lax.ppermute(a, 'sp', [(i, (i // rest ^ d) * rest + i % rest) for i in ra...]
    while x58 -> x0, local copies, waits for them, and re-layouts: 9.29 us -> none
    reduce_sum x10 -> x0, other arithmetic: 7.44 us -> none  [the longest x8 5.63 us: update(): mass = mass * factor + jnp.sum(expo, axis=-1)]
  transfers between devices with their start and end apart: 4 -> 15, of which waited for: 4 -> 9; matrix products, arithmetic and copies ran while one was open for 3% -> 6% of each run, Pallas kernels for 0% -> 28%
where the time goes in v1:
time: 92.6 us; the launch traced here: 92.3 us
  waiting for transfers between devices  32.8 us (35%)
  Pallas kernels  31 us (33%)
  starting transfers between devices  19.5 us (21%)
  local copies, waits for them, and re-layouts  7.26 us (8%)
  other arithmetic  1.6 us (2%)
    ppermute x6, waiting for transfers between devices, swap_far(): lax.ppermute(a, 'sp', [(i, (i // rest ^ d) * rest + i % rest) for i in ra...  18.3 us
    pallas_call x1, Pallas kernels, attend(): pl.pallas_call(functools.partial(attend_body, nq=nq, span=span, counts=co...  18.2 us
    ppermute x4, waiting for transfers between devices, swap_near(): return lax.ppermute(a, 'sp', [(i, i ^ d) for i in range(size)])  13.3 us
    ppermute x6, starting transfers between devices, swap_far(): lax.ppermute(a, 'sp', [(i, (i // rest ^ d) * rest + i % rest) for i in ra...  12.4 us
    pallas_call x1, Pallas kernels, project(): pl.pallas_call(project_body, grid_spec=pltpu.PrefetchScalarGridSpec(num_s...  7.73 us
    ppermute x4, starting transfers between devices, swap_near(): return lax.ppermute(a, 'sp', [(i, i ^ d) for i in range(size)])  6.09 us
    pallas_call x1, Pallas kernels, output(): pl.pallas_call(output_body, grid_spec=pltpu.PrefetchScalarGridSpec(num_sc...  5.03 us
    unnamed x32, local copies, waits for them, and re-layouts  3.49 us
  transfers between devices with their start and end apart: 15, of which 9 were waited for; matrix products, arithmetic and copies ran while one was open for 6% of the time, Pallas kernels for 28%

profile of v1, /device:TPU:0, one launch (start us, length us, event | category | flops | bytes accessed | tf_op | source)
XLA Modules:
  0.0 92.3 jit_solution(16994450386767592440)
XLA Ops:
  0.0 0.5 collective-permute-start.14
  0.5 0.5 fusion
  1.1 1.0 %pad_maximum_fusion.1 = (f32[256,128]{1,0:T(8,128)}, f32[256,128]{1,0:T(8,128)}) fusion(f32[256,32]{1,0:T(8,128)S(1)} %get-tuple-element.23, f32[256,32]{1,0:T(8,128)S(1)} %get-tuple-element.22, f32[256,32]{1,0:T(8,128)S(1)} %get-tuple-element.21), kind=kLoop, calls=%fused_computation.6 | loop fusion | flops 196608 | bytes 360448 | tf_op jit(solution)/shard_map/concatenate | solution.py:286
  2.0 7.7 %project.1 = (bf16[768,128]{1,0:T(8,128)(2,1)}, bf16[768,128]{1,0:T(8,128)(2,1)}, bf16[768,128]{1,0:T(8,128)(2,1)}, bf16[768,128]{1,0:T(8,128)(2,1)}) custom-call(s32[1]{0:T(128)} %bitcast.zi, bf16[256,2048]{1,0:T(8,128)(2,1)} %x.1, f32[1,2048]{1,0:T(1,128)} %bitcast.11, f32[256,128]{1,0:T(8,128)} %get-tuple-element.24.cosine, ...), custom_call_target="tpu_custom_call" | custom-call | tf_op jit(solution)/shard_map/project/pallas_call | solution.py:74
  9.8 2.6 %collective-permute-start = (bf16[768,128]{1,0:T(8,128)(2,1)}, bf16[768,128]{1,0:T(8,128)(2,1)S(1)}, u32[]{:S(2)}, u32[]{:S(2)}) collective-permute-start(bf16[768,128]{1,0:T(8,128)(2,1)} %get-tuple-element.14), channel_id=1, source_target_pairs={{0,8},{2,10},{4,12},{6,14},{8,0},{10,2},{12,4},{14,6},{16,24},{18,... | collective-permute-start | bytes 589832 | tf_op jit(solution)/shard_map/ppermute | solution.py:275
  12.4 2.6 %collective-permute-start.1 = (bf16[768,128]{1,0:T(8,128)(2,1)}, bf16[768,128]{1,0:T(8,128)(2,1)S(1)}, u32[]{:S(2)}, u32[]{:S(2)}) collective-permute-start(bf16[768,128]{1,0:T(8,128)(2,1)} %get-tuple-element.15), channel_id=1, source_target_pairs={{0,16},{2,18},{4,20},{6,22},{8,24},{10,26},{12,28},{14,30},{16,0},... | collective-permute-start | bytes 589832 | tf_op jit(solution)/shard_map/ppermute | solution.py:275
  15.0 0.9 slice_bitcast_fusion.3
  15.9 6.0 %collective-permute-done.refs_1_ = bf16[768,128]{1,0:T(8,128)(2,1)S(1)} collective-permute-done((bf16[768,128]{1,0:T(8,128)(2,1)}, bf16[768,128]{1,0:T(8,128)(2,1)S(1)}, u32[]{:S(2)}, u32[]{:S(2)}) %collective-permute-start) | collective-permute-done | bytes 196640 | tf_op jit(solution)/shard_map/ppermute | solution.py:275
  22.0 7.8 %collective-permute-done.1.refs_2_ = bf16[768,128]{1,0:T(8,128)(2,1)S(1)} collective-permute-done((bf16[768,128]{1,0:T(8,128)(2,1)}, bf16[768,128]{1,0:T(8,128)(2,1)S(1)}, u32[]{:S(2)}, u32[]{:S(2)}) %collective-permute-start.1) | collective-permute-done | bytes 196640 | tf_op jit(solution)/shard_map/ppermute | solution.py:275
  29.8 0.7 copy-done.6
  30.6 1.6 %collective-permute-start.4 = (bf16[4,512,128]{2,1,0:T(8,128)(2,1)S(1)}, bf16[4,512,128]{2,1,0:T(8,128)(2,1)S(1)}, u32[]{:S(2)}, u32[]{:S(2)}) collective-permute-start(bf16[4,512,128]{2,1,0:T(8,128)(2,1)S(1)} %pad_maximum_fusion.refs_4_), channel_id=1, source_target_pairs={{0,4},{2,6},{4,0},{6,2},{8,12},{10,14},{12,8},{14,10},{16,20},{18,... | collective-permute-start | bytes 1572872 | tf_op jit(solution)/shard_map/ppermute | solution.py:280
  32.2 1.5 %collective-permute-start.3 = (bf16[4,512,128]{2,1,0:T(8,128)(2,1)S(1)}, bf16[4,512,128]{2,1,0:T(8,128)(2,1)S(1)}, u32[]{:S(2)}, u32[]{:S(2)}) collective-permute-start(bf16[4,512,128]{2,1,0:T(8,128)(2,1)S(1)} %pad_maximum_fusion.refs_4_), channel_id=1, source_target_pairs={{0,2},{2,0},{4,6},{6,4},{8,10},{10,8},{12,14},{14,12},{16,18},{18,... | collective-permute-start | bytes 1572872 | tf_op jit(solution)/shard_map/ppermute | solution.py:280
  33.7 9.5 %collective-permute-done.4.refs_6_ = bf16[4,512,128]{2,1,0:T(8,128)(2,1)S(1)} collective-permute-done((bf16[4,512,128]{2,1,0:T(8,128)(2,1)S(1)}, bf16[4,512,128]{2,1,0:T(8,128)(2,1)S(1)}, u32[]{:S(2)}, u32[]{:S(2)}) %collective-permute-start.4) | collective-permute-done | bytes 524320 | tf_op jit(solution)/shard_map/ppermute | solution.py:280
  43.2 0.8 slice.28
  43.9 1.5 %collective-permute-start.6 = (bf16[2,512,128]{2,1,0:T(8,128)(2,1)}, bf16[2,512,128]{2,1,0:T(8,128)(2,1)}, u32[]{:S(2)}, u32[]{:S(2)}) collective-permute-start(bf16[2,512,128]{2,1,0:T(8,128)(2,1)} %slice.28), channel_id=1, source_target_pairs={{0,2},{2,0},{4,6},{6,4},{8,10},{10,8},{12,14},{14,12},{16,18},{18,... | collective-permute-start | bytes 786440 | tf_op jit(solution)/shard_map/ppermute | solution.py:280
  45.4 0.8 copy-done.3
  46.2 0.7 slice.27
  47.0 1.5 %collective-permute-start.5 = (bf16[2,512,128]{2,1,0:T(8,128)(2,1)}, bf16[2,512,128]{2,1,0:T(8,128)(2,1)}, u32[]{:S(2)}, u32[]{:S(2)}) collective-permute-start(bf16[2,512,128]{2,1,0:T(8,128)(2,1)} %slice.27), channel_id=1, source_target_pairs={{0,4},{2,6},{4,0},{6,2},{8,12},{10,14},{12,8},{14,10},{16,20},{18,... | collective-permute-start | bytes 786440 | tf_op jit(solution)/shard_map/ppermute | solution.py:280
  48.5 0.7 copy.11.refs_10_
  49.2 0.6 dynamic_slice.3.refs_9_
  49.8 0.8 collective-permute-done.6.refs_8_
  50.6 3.0 %collective-permute-done.5.refs_7_ = bf16[2,512,128]{2,1,0:T(8,128)(2,1)} collective-permute-done((bf16[2,512,128]{2,1,0:T(8,128)(2,1)}, bf16[2,512,128]{2,1,0:T(8,128)(2,1)}, u32[]{:S(2)}, u32[]{:S(2)}) %collective-permute-start.5) | collective-permute-done | bytes 262176 | tf_op jit(solution)/shard_map/ppermute | solution.py:280
  53.7 18.2 %attend.1 = (bf16[256,128]{1,0:T(8,128)(2,1)}, bf16[256,128]{1,0:T(8,128)(2,1)}, bf16[256,128]{1,0:T(8,128)(2,1)}, bf16[256,128]{1,0:T(8,128)(2,1)}) custom-call(bf16[768,128]{1,0:T(8,128)(2,1)} %get-tuple-element.13.refs_0_, bf16[768,128]{1,0:T(8,128)(2,1)} %copy-done.4, bf16[768,128]{1,0:T(8,128)(2,1)} %copy-done.5, bf16[768,128]{1,0:T(8,128)(2,1)} %copy-done.6, ...), custom_call_target="tpu_custom_call" | custom-call | tf_op jit(solution)/shard_map/attend/pallas_call | solution.py:206
  71.9 4.8 %collective-permute-start.7 = (bf16[256,128]{1,0:T(8,128)(2,1)}, bf16[256,128]{1,0:T(8,128)(2,1)S(1)}, u32[]{:S(2)}, u32[]{:S(2)}) collective-permute-start(bf16[256,128]{1,0:T(8,128)(2,1)} %get-tuple-element.18), channel_id=1, source_target_pairs={{0,8},{2,10},{4,12},{6,14},{8,0},{10,2},{12,4},{14,6},{16,24},{18,... | collective-permute-start | bytes 196616 | tf_op jit(solution)/shard_map/ppermute | solution.py:275
  76.6 1.0 %collective-permute-start.8 = (bf16[256,128]{1,0:T(8,128)(2,1)}, bf16[256,128]{1,0:T(8,128)(2,1)S(1)}, u32[]{:S(2)}, u32[]{:S(2)}) collective-permute-start(bf16[256,128]{1,0:T(8,128)(2,1)} %get-tuple-element.19), channel_id=1, source_target_pairs={{0,16},{2,18},{4,20},{6,22},{8,24},{10,26},{12,28},{14,30},{16,0},... | collective-permute-start | bytes 196616 | tf_op jit(solution)/shard_map/ppermute | solution.py:275
  77.6 1.5 %collective-permute-start.9 = (bf16[256,128]{1,0:T(8,128)(2,1)}, bf16[256,128]{1,0:T(8,128)(2,1)S(1)}, u32[]{:S(2)}, u32[]{:S(2)}) collective-permute-start(bf16[256,128]{1,0:T(8,128)(2,1)} %get-tuple-element.20), channel_id=1, source_target_pairs={{0,24},{2,26},{4,28},{6,30},{8,16},{10,18},{12,20},{14,22},{16,8},... | collective-permute-start | bytes 196616 | tf_op jit(solution)/shard_map/ppermute | solution.py:275
  79.6 3.1 %collective-permute-done.8.refs_2_ = bf16[256,128]{1,0:T(8,128)(2,1)S(1)} collective-permute-done((bf16[256,128]{1,0:T(8,128)(2,1)}, bf16[256,128]{1,0:T(8,128)(2,1)S(1)}, u32[]{:S(2)}, u32[]{:S(2)}) %collective-permute-start.8) | collective-permute-done | bytes 65568 | tf_op jit(solution)/shard_map/ppermute | solution.py:275
  82.7 1.3 %collective-permute-done.9.refs_3_ = bf16[256,128]{1,0:T(8,128)(2,1)S(1)} collective-permute-done((bf16[256,128]{1,0:T(8,128)(2,1)}, bf16[256,128]{1,0:T(8,128)(2,1)S(1)}, u32[]{:S(2)}, u32[]{:S(2)}) %collective-permute-start.9) | collective-permute-done | bytes 65568 | tf_op jit(solution)/shard_map/ppermute | solution.py:275
  84.1 1.2 %collective-permute-done.13.refs_7_ = bf16[256,128]{1,0:T(8,128)(2,1)S(1)} collective-permute-done((bf16[256,128]{1,0:T(8,128)(2,1)S(1)}, bf16[256,128]{1,0:T(8,128)(2,1)S(1)}, u32[]{:S(2)}, u32[]{:S(2)}) %collective-permute-start.13) | collective-permute-done | bytes 65568 | tf_op jit(solution)/shard_map/ppermute | solution.py:328
  85.3 0.6 copy-done.13
  85.9 1.3 %copy-done = bf16[512,2048]{1,0:T(8,128)(2,1)} copy-done((bf16[512,2048]{1,0:T(8,128)(2,1)}, bf16[512,2048]{1,0:T(8,128)(2,1)S(1)}, u32[]{:S(2)}) %copy-start) | copy-done | bytes 2097176
  87.2 5.0 %output.1 = bf16[256,2048]{1,0:T(8,128)(2,1)} custom-call(s32[1]{0:T(128)} %bitcast.zi, bf16[256,128]{1,0:T(8,128)(2,1)} %get-tuple-element.17.refs_0_, bf16[256,128]{1,0:T(8,128)(2,1)} %copy-done.7, bf16[256,128]{1,0:T(8,128)(2,1)} %copy-done.8, bf16[256,128]{1,0:T(8,128)(2,1)} %copy-done.9, bf16[256,128]{1,0:T(8,128)(2,1)} %copy-done.10, ...), custom_call_target="tpu_custom_call" | custom-call | tf_op jit(solution)/shard_map/output/pallas_call | solution.py:249
  (46 shorter events, 0.7 us)
Async XLA Ops:
  0.0 85.3 %collective-permute-start.14 = (bf16[512,2048]{1,0:T(8,128)(2,1)}, bf16[512,2048]{1,0:T(8,128)(2,1)S(1)}, u32[]{:S(2)}, u32[]{:S(2)}) collective-permute-start(bf16[512,2048]{1,0:T(8,128)(2,1)} %refs_8_.1), channel_id=1, source_target_pairs={{0,1},{1,0},{2,3},{3,2},{4,5},{5,4},{6,7},{7,6},{8,9},{9,8},{10,11... | collective-permute-start | bytes 6291464 | tf_op jit(solution)/shard_map/ppermute | solution.py:327
  9.8 38.7 %copy-start.14 = (f32[128]{0:T(128)S(1)}, f32[128]{0:T(128)}, u32[]{:S(2)}) copy-start(f32[128]{0:T(128)} %param.14) | copy-start | bytes 1540
  9.8 39.5 %copy-start.15 = (f32[4]{0:T(128)S(1)}, f32[4]{0:T(128)}, u32[]{:S(2)}) copy-start(f32[4]{0:T(128)} %param.13) | copy-start | bytes 52
  9.8 12.2 %collective-permute-start = (bf16[768,128]{1,0:T(8,128)(2,1)}, bf16[768,128]{1,0:T(8,128)(2,1)S(1)}, u32[]{:S(2)}, u32[]{:S(2)}) collective-permute-start(bf16[768,128]{1,0:T(8,128)(2,1)} %get-tuple-element.14), channel_id=1, source_target_pairs={{0,8},{2,10},{4,12},{6,14},{8,0},{10,2},{12,4},{14,6},{16,24},{18,... | collective-permute-start | bytes 589832 | tf_op jit(solution)/shard_map/ppermute | solution.py:275
  12.4 17.4 %collective-permute-start.1 = (bf16[768,128]{1,0:T(8,128)(2,1)}, bf16[768,128]{1,0:T(8,128)(2,1)S(1)}, u32[]{:S(2)}, u32[]{:S(2)}) collective-permute-start(bf16[768,128]{1,0:T(8,128)(2,1)} %get-tuple-element.15), channel_id=1, source_target_pairs={{0,16},{2,18},{4,20},{6,22},{8,24},{10,26},{12,28},{14,30},{16,0},... | collective-permute-start | bytes 589832 | tf_op jit(solution)/shard_map/ppermute | solution.py:275
  15.0 14.8 %collective-permute-start.2 = (bf16[768,128]{1,0:T(8,128)(2,1)}, bf16[768,128]{1,0:T(8,128)(2,1)S(1)}, u32[]{:S(2)}, u32[]{:S(2)}) collective-permute-start(bf16[768,128]{1,0:T(8,128)(2,1)} %get-tuple-element.16), channel_id=1, source_target_pairs={{0,24},{2,26},{4,28},{6,30},{8,16},{10,18},{12,20},{14,22},{16,8},... | collective-permute-start | bytes 589832 | tf_op jit(solution)/shard_map/ppermute | solution.py:275
  22.0 31.7 %copy-start.4 = (bf16[768,128]{1,0:T(8,128)(2,1)}, bf16[768,128]{1,0:T(8,128)(2,1)S(1)}, u32[]{:S(2)}) copy-start(bf16[768,128]{1,0:T(8,128)(2,1)S(1)} %collective-permute-done.refs_1_) | copy-start | bytes 589828
  29.8 23.9 %copy-start.5 = (bf16[768,128]{1,0:T(8,128)(2,1)}, bf16[768,128]{1,0:T(8,128)(2,1)S(1)}, u32[]{:S(2)}) copy-start(bf16[768,128]{1,0:T(8,128)(2,1)S(1)} %collective-permute-done.1.refs_2_) | copy-start | bytes 589828
  29.8 0.7 copy-start.6
  30.6 23.0 %copy-start.1 = (bf16[4,512,128]{2,1,0:T(8,128)(2,1)}, bf16[4,512,128]{2,1,0:T(8,128)(2,1)S(1)}, u32[]{:S(2)}) copy-start(bf16[4,512,128]{2,1,0:T(8,128)(2,1)S(1)} %pad_maximum_fusion.refs_4_) | copy-start | bytes 1572868
  30.6 12.5 %collective-permute-start.4 = (bf16[4,512,128]{2,1,0:T(8,128)(2,1)S(1)}, bf16[4,512,128]{2,1,0:T(8,128)(2,1)S(1)}, u32[]{:S(2)}, u32[]{:S(2)}) collective-permute-start(bf16[4,512,128]{2,1,0:T(8,128)(2,1)S(1)} %pad_maximum_fusion.refs_4_), channel_id=1, source_target_pairs={{0,4},{2,6},{4,0},{6,2},{8,12},{10,14},{12,8},{14,10},{16,20},{18,... | collective-permute-start | bytes 1572872 | tf_op jit(solution)/shard_map/ppermute | solution.py:280
  32.2 13.2 %collective-permute-start.3 = (bf16[4,512,128]{2,1,0:T(8,128)(2,1)S(1)}, bf16[4,512,128]{2,1,0:T(8,128)(2,1)S(1)}, u32[]{:S(2)}, u32[]{:S(2)}) collective-permute-start(bf16[4,512,128]{2,1,0:T(8,128)(2,1)S(1)} %pad_maximum_fusion.refs_4_), channel_id=1, source_target_pairs={{0,2},{2,0},{4,6},{6,4},{8,10},{10,8},{12,14},{14,12},{16,18},{18,... | collective-permute-start | bytes 1572872 | tf_op jit(solution)/shard_map/ppermute | solution.py:280
  43.2 10.5 %copy-start.2 = (bf16[4,512,128]{2,1,0:T(8,128)(2,1)}, bf16[4,512,128]{2,1,0:T(8,128)(2,1)S(1)}, u32[]{:S(2)}) copy-start(bf16[4,512,128]{2,1,0:T(8,128)(2,1)S(1)} %collective-permute-done.4.refs_6_) | copy-start | bytes 1572868
  43.9 6.7 %collective-permute-start.6 = (bf16[2,512,128]{2,1,0:T(8,128)(2,1)}, bf16[2,512,128]{2,1,0:T(8,128)(2,1)}, u32[]{:S(2)}, u32[]{:S(2)}) collective-permute-start(bf16[2,512,128]{2,1,0:T(8,128)(2,1)} %slice.28), channel_id=1, source_target_pairs={{0,2},{2,0},{4,6},{6,4},{8,10},{10,8},{12,14},{14,12},{16,18},{18,... | collective-permute-start | bytes 786440 | tf_op jit(solution)/shard_map/ppermute | solution.py:280
  45.4 0.8 copy-start.3
  47.0 6.7 %collective-permute-start.5 = (bf16[2,512,128]{2,1,0:T(8,128)(2,1)}, bf16[2,512,128]{2,1,0:T(8,128)(2,1)}, u32[]{:S(2)}, u32[]{:S(2)}) collective-permute-start(bf16[2,512,128]{2,1,0:T(8,128)(2,1)} %slice.27), channel_id=1, source_target_pairs={{0,4},{2,6},{4,0},{6,2},{8,12},{10,14},{12,8},{14,10},{16,20},{18,... | collective-permute-start | bytes 786440 | tf_op jit(solution)/shard_map/ppermute | solution.py:280
  71.9 7.3 %collective-permute-start.7 = (bf16[256,128]{1,0:T(8,128)(2,1)}, bf16[256,128]{1,0:T(8,128)(2,1)S(1)}, u32[]{:S(2)}, u32[]{:S(2)}) collective-permute-start(bf16[256,128]{1,0:T(8,128)(2,1)} %get-tuple-element.18), channel_id=1, source_target_pairs={{0,8},{2,10},{4,12},{6,14},{8,0},{10,2},{12,4},{14,6},{16,24},{18,... | collective-permute-start | bytes 196616 | tf_op jit(solution)/shard_map/ppermute | solution.py:275
  76.6 6.1 %collective-permute-start.8 = (bf16[256,128]{1,0:T(8,128)(2,1)}, bf16[256,128]{1,0:T(8,128)(2,1)S(1)}, u32[]{:S(2)}, u32[]{:S(2)}) collective-permute-start(bf16[256,128]{1,0:T(8,128)(2,1)} %get-tuple-element.19), channel_id=1, source_target_pairs={{0,16},{2,18},{4,20},{6,22},{8,24},{10,26},{12,28},{14,30},{16,0},... | collective-permute-start | bytes 196616 | tf_op jit(solution)/shard_map/ppermute | solution.py:275
  77.6 6.4 %collective-permute-start.9 = (bf16[256,128]{1,0:T(8,128)(2,1)}, bf16[256,128]{1,0:T(8,128)(2,1)S(1)}, u32[]{:S(2)}, u32[]{:S(2)}) collective-permute-start(bf16[256,128]{1,0:T(8,128)(2,1)} %get-tuple-element.20), channel_id=1, source_target_pairs={{0,24},{2,26},{4,28},{6,30},{8,16},{10,18},{12,20},{14,22},{16,8},... | collective-permute-start | bytes 196616 | tf_op jit(solution)/shard_map/ppermute | solution.py:275
  79.1 4.9 %collective-permute-start.10 = (bf16[256,128]{1,0:T(8,128)(2,1)}, bf16[256,128]{1,0:T(8,128)(2,1)S(1)}, u32[]{:S(2)}, u32[]{:S(2)}) collective-permute-start(bf16[256,128]{1,0:T(8,128)(2,1)} %get-tuple-element.17.refs_0_), channel_id=1, source_target_pairs={{0,1},{1,0},{2,3},{3,2},{4,5},{5,4},{6,7},{7,6},{8,9},{9,8},{10,11... | collective-permute-start | bytes 196616 | tf_op jit(solution)/shard_map/ppermute | solution.py:328
  79.2 6.1 %copy-start.7 = (bf16[256,128]{1,0:T(8,128)(2,1)}, bf16[256,128]{1,0:T(8,128)(2,1)S(1)}, u32[]{:S(2)}) copy-start(bf16[256,128]{1,0:T(8,128)(2,1)S(1)} %collective-permute-done.7.refs_1_) | copy-start | bytes 196612
  79.2 4.8 %collective-permute-start.11 = (bf16[256,128]{1,0:T(8,128)(2,1)S(1)}, bf16[256,128]{1,0:T(8,128)(2,1)S(1)}, u32[]{:S(2)}, u32[]{:S(2)}) collective-permute-start(bf16[256,128]{1,0:T(8,128)(2,1)S(1)} %collective-permute-done.7.refs_1_), channel_id=1, source_target_pairs={{0,1},{1,0},{2,3},{3,2},{4,5},{5,4},{6,7},{7,6},{8,9},{9,8},{10,11... | collective-permute-start | bytes 196616 | tf_op jit(solution)/shard_map/ppermute | solution.py:328
  82.7 2.6 %copy-start.8 = (bf16[256,128]{1,0:T(8,128)(2,1)}, bf16[256,128]{1,0:T(8,128)(2,1)S(1)}, u32[]{:S(2)}) copy-start(bf16[256,128]{1,0:T(8,128)(2,1)S(1)} %collective-permute-done.8.refs_2_) | copy-start | bytes 196612
  82.7 1.3 %collective-permute-start.12 = (bf16[256,128]{1,0:T(8,128)(2,1)S(1)}, bf16[256,128]{1,0:T(8,128)(2,1)S(1)}, u32[]{:S(2)}, u32[]{:S(2)}) collective-permute-start(bf16[256,128]{1,0:T(8,128)(2,1)S(1)} %collective-permute-done.8.refs_2_), channel_id=1, source_target_pairs={{0,1},{1,0},{2,3},{3,2},{4,5},{5,4},{6,7},{7,6},{8,9},{9,8},{10,11... | collective-permute-start | bytes 196616 | tf_op jit(solution)/shard_map/ppermute | solution.py:328
  84.0 1.3 %copy-start.9 = (bf16[256,128]{1,0:T(8,128)(2,1)}, bf16[256,128]{1,0:T(8,128)(2,1)S(1)}, u32[]{:S(2)}) copy-start(bf16[256,128]{1,0:T(8,128)(2,1)S(1)} %collective-permute-done.9.refs_3_) | copy-start | bytes 196612
  84.0 1.3 %collective-permute-start.13 = (bf16[256,128]{1,0:T(8,128)(2,1)S(1)}, bf16[256,128]{1,0:T(8,128)(2,1)S(1)}, u32[]{:S(2)}, u32[]{:S(2)}) collective-permute-start(bf16[256,128]{1,0:T(8,128)(2,1)S(1)} %collective-permute-done.9.refs_3_), channel_id=1, source_target_pairs={{0,1},{1,0},{2,3},{3,2},{4,5},{5,4},{6,7},{7,6},{8,9},{9,8},{10,11... | collective-permute-start | bytes 196616 | tf_op jit(solution)/shard_map/ppermute | solution.py:328
  84.0 1.3 %copy-start.10 = (bf16[256,128]{1,0:T(8,128)(2,1)}, bf16[256,128]{1,0:T(8,128)(2,1)S(1)}, u32[]{:S(2)}) copy-start(bf16[256,128]{1,0:T(8,128)(2,1)S(1)} %collective-permute-done.10.refs_4_) | copy-start | bytes 196612
  84.0 1.3 %copy-start.11 = (bf16[256,128]{1,0:T(8,128)(2,1)}, bf16[256,128]{1,0:T(8,128)(2,1)S(1)}, u32[]{:S(2)}) copy-start(bf16[256,128]{1,0:T(8,128)(2,1)S(1)} %collective-permute-done.11.refs_5_) | copy-start | bytes 196612
  84.1 1.3 %copy-start.12 = (bf16[256,128]{1,0:T(8,128)(2,1)}, bf16[256,128]{1,0:T(8,128)(2,1)S(1)}, u32[]{:S(2)}) copy-start(bf16[256,128]{1,0:T(8,128)(2,1)S(1)} %collective-permute-done.12.refs_6_) | copy-start | bytes 196612
  85.3 0.6 copy-start.13
  85.9 1.4 %copy-start = (bf16[512,2048]{1,0:T(8,128)(2,1)}, bf16[512,2048]{1,0:T(8,128)(2,1)S(1)}, u32[]{:S(2)}) copy-start(bf16[512,2048]{1,0:T(8,128)(2,1)S(1)} %collective-permute-done.14.refs_9_) | copy-start | bytes 6291460

commit v2 on v1

--- a/solution.py
+++ b/solution.py
@@ -105,7 +105,6 @@
     extra = take(2) if last else []
     outs = take(nq) if last else take(3)
     kscr, vscr, qscr, sscr = take(4)
-    blocks = 2 * nq
     total = sum(counts)
     pair = vscr.shape[2] // span
     step = pair * span
@@ -127,62 +126,54 @@
         zero = jnp.zeros_like(high)
         for c in range(2):
             mask = row if c == 0 else jnp.logical_not(row)
-            qscr[2 * d + c, 0 : 2 * KD] = jnp.where(mask, high, zero)
-            qscr[2 * d + c, 2 * KD : 4 * KD] = jnp.where(mask, rest, zero)
+            cols = slice(c * span, (c + 1) * span)
+            qscr[d, 0 : 2 * KD, cols] = jnp.where(mask, high, zero)
+            qscr[d, 2 * KD : 4 * KD, cols] = jnp.where(mask, rest, zero)
 
     def groups(a):
         return a.reshape(a.shape[0] // 8, 8, a.shape[1])
 
-    def score(b, slot, i, m8):
-        k = kscr[pl.ds(pl.multiple_of(i * step, step), step), :]
-        s = jnp.dot(jnp.concatenate([k, k], axis=1), qscr[b], preferred_element_type=F32)
-        sscr[slot, pl.ds(pl.multiple_of(i * step, step), step), :] = s
+    def score(d, i, m8):
+        k = kscr[i * step : (i + 1) * step, :]
+        s = jnp.dot(jnp.concatenate([k, k], axis=1), qscr[d], preferred_element_type=F32)
+        sscr[d % 2, i * step : (i + 1) * step, :] = s
         return jnp.maximum(m8, jnp.max(groups(s), axis=0))
 
-    def spread(m8):
-        return jnp.broadcast_to(jnp.max(m8, axis=0, keepdims=True), m8.shape)
-
-    low = jnp.full((8, span), -1e30, F32)
-    zero8 = jnp.zeros((8, span), F32)
-    state = []
-    m8 = lax.fori_loop(0, steps, lambda i, m: score(0, 0, i, m), low if first else carry_in[0][0])
-    for b in range(blocks):
-        m = spread(m8)
+    low = jnp.full((8, 2 * span), -1e30, F32)
+    m8 = low if first else carry_in[0][0]
+    for i in range(steps):
+        m8 = score(0, i, m8)
+    for d in range(nq):
+        m = jnp.broadcast_to(jnp.max(m8, axis=0, keepdims=True), m8.shape)
         if first:
-            mass0 = zero8
-            acc0 = jnp.zeros((VD, span), F32)
+            mass = jnp.zeros_like(m)
+            acc = None
         else:
-            fix = jnp.exp2(carry_in[0][b] - m)
-            mass0 = carry_in[1][b] * fix
-            acc0 = (groups(carry_in[2][b]) * fix[None]).reshape(VD, span)
-
-        def body(i, carry, b=b, m=m):
-            next8, mass, acc = carry
-            s = sscr[b % 2, pl.ds(pl.multiple_of(i * step, step), step), :]
-            p = jnp.exp2(groups(s) - m[None])
+            fix = jnp.exp2(carry_in[0][d] - m)
+            mass = carry_in[1][d] * fix
+            acc = (groups(carry_in[2][d]) * fix[None]).reshape(VD, 2 * span)
+        more = d + 1 < nq
+        if more:
+            m8 = low if first else carry_in[0][d + 1]
+        for i in range(steps):
+            p = jnp.exp2(groups(sscr[d % 2, i * step : (i + 1) * step, :]) - m[None])
             mass = mass + jnp.sum(p, axis=0)
-            acc = acc + jnp.dot(
-                vscr[i], p.reshape(step, span).astype(BF16), preferred_element_type=F32
+            part = jnp.dot(
+                vscr[i], p.reshape(step, 2 * span).astype(BF16), preferred_element_type=F32
             )
-            if b + 1 < blocks:
-                next8 = score(b + 1, (b + 1) % 2, i, next8)
-            return next8, mass, acc
-
-        next0 = low if first or b + 1 == blocks else carry_in[0][b + 1]
-        m8, mass, acc = lax.fori_loop(0, steps, body, (next0, mass0, acc0))
+            acc = part if acc is None else acc + part
+            if more:
+                m8 = score(d + 1, i, m8)
         if not last:
-            outs[0][b] = m
-            outs[1][b] = mass
-            outs[2][b] = acc
+            outs[0][d] = m
+            outs[1][d] = mass
+            outs[2][d] = acc
             continue
+        lam, gain = extra
         read = acc / jnp.sum(mass, axis=0, keepdims=True)
-        if b % 2 == 0:
-            state = read
-        else:
-            lam, gain = extra
-            diff = state - lam[0] * read
-            inv = lax.rsqrt(jnp.mean(diff * diff, axis=0, keepdims=True) + 1e-05)
-            outs[b // 2][...] = (diff * inv * gain[...]).T.astype(BF16)
+        diff = read[:, :span] - lam[0] * read[:, span:]
+        inv = lax.rsqrt(jnp.mean(diff * diff, axis=0, keepdims=True) + 1e-05)
+        outs[d][...] = (diff * inv * gain[...]).T.astype(BF16)
 
 
 def attend(qs, kvs, carry, finish, span):
@@ -190,7 +181,6 @@
     counts = tuple(kv.shape[0] for kv in kvs)
     total = sum(counts)
     pair = next(n for n in (4, 2, 1) if total % n == 0)
-    blocks = 2 * nq
     first, last = carry is None, finish is not None
     args = [*qs, *kvs, *(carry or ()), *(finish or ())]
     specs = [whole_spec() for _ in args]
@@ -199,9 +189,9 @@
         out_shape = [jax.ShapeDtypeStruct((span, VD), BF16)] * nq
     else:
         out_shape = [
-            jax.ShapeDtypeStruct((blocks, 8, span), F32),
-            jax.ShapeDtypeStruct((blocks, 8, span), F32),
-            jax.ShapeDtypeStruct((blocks, VD, span), F32),
+            jax.ShapeDtypeStruct((nq, 8, 2 * span), F32),
+            jax.ShapeDtypeStruct((nq, 8, 2 * span), F32),
+            jax.ShapeDtypeStruct((nq, VD, 2 * span), F32),
         ]
     return pl.pallas_call(
         functools.partial(
@@ -213,8 +203,8 @@
         scratch_shapes=[
             pltpu.VMEM((total * span, VD), BF16),
             pltpu.VMEM((total // pair, VD, pair * span), BF16),
-            pltpu.VMEM((blocks, 4 * KD, span), BF16),
-            pltpu.VMEM((2, total * span, span), F32),
+            pltpu.VMEM((nq, 4 * KD, 2 * span), BF16),
+            pltpu.VMEM((2, total * span, 2 * span), F32),
         ],
         compiler_params=pltpu.CompilerParams(vmem_limit_bytes=VMEM_LIMIT),
         name="attend",
@@ -269,6 +259,7 @@
     split = heads if heads & (heads - 1) == 0 and size % heads == 0 else 1
     rest = size // split
     where = lax.axis_index("sp")
+    flip = [(0, 1), (1, 0)]
     zi = where // rest
 
     def swap_far(a, d):
@@ -290,42 +281,74 @@
     gain = sub_gain[:, None]
 
     if split == heads:
-        mine = [parts[0]] + [None] * (heads - 1)
-        for d in sorted(range(1, heads), key=lambda n: -(n ^ 1)):
-            mine[d] = swap_far(parts[d], d)
-        kv = jnp.stack([a[: 2 * span] for a in mine])
-        if rest == 4:
-            half = heads // 2 if heads > 1 else 1
-            left, right = swap_near(kv, 1), swap_near(kv, 2)
-            cross = [swap_near(left[:half], 2)]
-            if heads > 1:
-                cross.append(swap_near(right[half:], 1))
-            pieces = [[kv, left, right, *cross]]
+        swapped = tp == 2 and rest == 4
+        lam_here = lam
+        if swapped:
+            lam_other = lax.ppermute(lam, "tp", flip)
+            same = (where % 4) // 2 == lax.axis_index("tp")
+            lam_here = jnp.where(same, lam, lam_other)
+
+            def far(a, d):
+                pairs = []
+                for i in range(size):
+                    z, y, x = i // 4, (i // 2) % 2, i % 2
+                    for t in range(2):
+                        pairs.append((2 * i + t, 2 * ((z ^ d) * 4 + t * 2 + x) + y))
+                return lax.ppermute(a, ("sp", "tp"), pairs)
+
+            mine = [None] * heads
+            for d in [0] + sorted(range(1, heads), key=lambda n: -(n ^ 1)):
+                mine[d] = far(parts[d], d)
         else:
+            far = swap_far
+            mine = [parts[0]] + [far(parts[d], d) for d in range(1, heads)]
+        lam_mine = lax.dynamic_slice_in_dim(lam_here, index[0], 1)
+        kv = [a[None, : 2 * span] for a in mine]
+        finish = (lam_mine, gain)
+        if swapped and heads == 4:
+            cross_core = lambda a: lax.ppermute(a, "tp", flip)
+            one = jnp.concatenate([kv[0], kv[2]], axis=0)
+            two = jnp.concatenate([kv[3], kv[1]], axis=0)
+            far_one = swap_near(one, 1)
+            far_two = swap_near(two, 1)
+            side_one, side_two = cross_core(one), cross_core(two)
+            far_side_one = cross_core(far_one)
+            far_side_two = cross_core(far_two)
+            carry = attend(mine, [one, two], None, None, span)
+            carry = attend(mine, [side_one, side_two], carry, None, span)
+            carry = attend(mine, [far_one, far_side_one], carry, None, span)
+            own = [None] * 4
+            for picks in ([2, 3], [1, 0]):
+                some = [
+                    jnp.concatenate([c[n : n + 1] for n in picks], axis=0) for c in carry
+                ]
+                done = attend([mine[n] for n in picks], [far_two, far_side_two], some, finish, span)
+                for n, a in zip(picks, done):
+                    own[n] = far(a, n)
+        else:
+            kv = jnp.concatenate(kv, axis=0)
             groups = [[g * rest + r for r in range(rest)] for g in range(split)]
             kw = {} if split == 1 else {"axis_index_groups": groups}
             every = lax.all_gather(kv, "sp", axis=0, tiled=True, **kw)
-            pieces = [[every[at : at + 16]] for at in range(0, every.shape[0], 16)]
-        lam_mine = lax.dynamic_slice_in_dim(lam, index[0], 1)
-        carry = None
-        for at, piece in enumerate(pieces):
-            finish = (lam_mine, gain) if at + 1 == len(pieces) else None
-            carry = attend(mine, piece, carry, finish, span)
-        own = [carry[0]] + [swap_far(carry[d], d) for d in range(1, heads)]
+            carry = None
+            for at in range(0, every.shape[0], 8):
+                end = finish if at + 8 >= every.shape[0] else None
+                carry = attend(mine, [every[at : at + 8]], carry, end, span)
+            own = [carry[0]] + [far(carry[d], d) for d in range(1, heads)]
     else:
         own = []
         for h in range(heads):
             every = lax.all_gather(parts[h][None, : 2 * span], "sp", axis=0, tiled=True)
             carry = None
-            for at in range(0, size, 16):
-                finish = (lam[h : h + 1], gain) if at + 16 >= size else None
-                carry = attend([parts[h]], [every[at : at + 16]], carry, finish, span)
+            for at in range(0, size, 8):
+                end = (lam[h : h + 1], gain) if at + 8 >= size else None
+                carry = attend([parts[h]], [every[at : at + 8]], carry, end, span)
             own.append(carry[0])
 
     if tp == 2:
-        flip = [(0, 1), (1, 0)]
         w_other = lax.ppermute(w_out, "tp", flip)
-        other = [lax.ppermute(a, "tp", flip) for a in own]
+        other = lax.ppermute(jnp.stack(own), "tp", flip)
+        other = [other[d] for d in range(heads)]
         return output(index, own, other, w_out, w_other)
     attended = jnp.concatenate(own, axis=1)
     if tp > 1:

time: 92.6 us -> 94.7 us (1.023)
  waiting for transfers between devices: 32.8 us -> 21.2 us
  Pallas kernels: 31 us -> 39.9 us
  starting transfers between devices: 19.5 us -> 22 us
  other arithmetic: 1.6 us -> 3.7 us
    ppermute x4 -> x2, waiting for transfers between devices: 13.3 us -> 2.67 us  [swap_near(): return lax.ppermute(a, 'sp', [(i, i ^ d) for i in range(size)])]
    pallas_call x1 -> x5, Pallas kernels: 18.2 us -> 27.1 us  [attend(): pl.pallas_call(functools.partial(attend_body, nq=nq, span=span, counts=co...]
    ppermute x10 -> x14, starting transfers between devices: 12.9 us -> 17.7 us  [the longest x8 14.2 us: far(): return lax.ppermute(a, ('sp', 'tp'), pairs)]
    concatenate x0 -> x3, local copies, waits for them, and re-layouts: none -> 4.72 us  [shards(): some = [jnp.concatenate([c[n:n + 1] for n in picks], axis=0) for c in carry]]
    unnamed x32, local copies, waits for them, and re-layouts: 3.49 us -> 0.06 us
    ppermute x4 -> x2, starting transfers between devices: 6.09 us -> 3.78 us  [swap_near(): return lax.ppermute(a, 'sp', [(i, i ^ d) for i in range(size)])]
    concatenate x0 -> x5, other arithmetic: none -> 2.11 us  [the longest x3 2.05 us: shards(): some = [jnp.concatenate([c[n:n + 1] for n in picks], axis=0) for c in carry]]
    slice x2 -> x3, local copies, waits for them, and re-layouts: 1.5 us -> 0.04 us  [shards(): some = [jnp.concatenate([c[n:n + 1] for n in picks], axis=0) for c in carry]]
  transfers between devices with their start and end apart: 15 -> 17, of which waited for: 9 -> 6; matrix products, arithmetic and copies ran while one was open for 6% -> 10% of each run, Pallas kernels for 28% -> 29%
where the time goes in v2:
time: 94.7 us; the launch traced here: 94 us
  Pallas kernels  39.9 us (42%)
  starting transfers between devices  22 us (23%)
  waiting for transfers between devices  21.2 us (22%)
  local copies, waits for them, and re-layouts  6.93 us (7%)
  other arithmetic  3.7 us (4%)
    pallas_call x5, Pallas kernels, attend(): pl.pallas_call(functools.partial(attend_body, nq=nq, span=span, counts=co...  27.1 us
    ppermute x8, starting transfers between devices, far(): return lax.ppermute(a, ('sp', 'tp'), pairs)  14.2 us
    ppermute x8, waiting for transfers between devices, far(): return lax.ppermute(a, ('sp', 'tp'), pairs)  14 us
    pallas_call x1, Pallas kernels, project(): pl.pallas_call(project_body, grid_spec=pltpu.PrefetchScalarGridSpec(num_s...  7.76 us
    pallas_call x1, Pallas kernels, output(): pl.pallas_call(output_body, grid_spec=pltpu.PrefetchScalarGridSpec(num_sc...  5 us
    concatenate x3, local copies, waits for them, and re-layouts, shards(): some = [jnp.concatenate([c[n:n + 1] for n in picks], axis=0) for c in carry]  4.72 us
    ppermute x2, starting transfers between devices, swap_near(): return lax.ppermute(a, 'sp', [(i, i ^ d) for i in range(size)])  3.78 us
    ppermute x1, waiting for transfers between devices, shards(): lam_other = lax.ppermute(lam, 'tp', flip)  3.4 us
  transfers between devices with their start and end apart: 17, of which 6 were waited for; matrix products, arithmetic and copies ran while one was open for 10% of the time, Pallas kernels for 29%

profile of v2, /device:TPU:0, one launch (start us, length us, event | category | flops | bytes accessed | tf_op | source)
XLA Modules:
  0.0 94.0 jit_solution(6830351459572152443)
XLA Ops:
  0.6 1.0 %pad_maximum_fusion.4 = (f32[256,128]{1,0:T(8,128)}, f32[256,128]{1,0:T(8,128)}) fusion(f32[256,32]{1,0:T(8,128)S(1)} %get-tuple-element.51, f32[256,32]{1,0:T(8,128)S(1)} %get-tuple-element.50, f32[256,32]{1,0:T(8,128)S(1)} %get-tuple-element.49), kind=kLoop, calls=%fused_computation.10 | loop fusion | flops 196608 | bytes 360448 | tf_op jit(solution)/shard_map/concatenate | solution.py:277
  1.6 7.8 %project.1 = (bf16[768,128]{1,0:T(8,128)(2,1)}, bf16[768,128]{1,0:T(8,128)(2,1)}, bf16[768,128]{1,0:T(8,128)(2,1)}, bf16[768,128]{1,0:T(8,128)(2,1)}) custom-call(s32[1]{0:T(128)} %bitcast.zi, bf16[256,2048]{1,0:T(8,128)(2,1)} %x.1, f32[1,2048]{1,0:T(1,128)} %bitcast.27, f32[256,128]{1,0:T(8,128)} %get-tuple-element.52.cosine, ...), custom_call_target="tpu_custom_call" | custom-call | tf_op jit(solution)/shard_map/project/pallas_call | solution.py:74
  9.4 4.1 %collective-permute-start.5 = (bf16[768,128]{1,0:T(8,128)(2,1)}, bf16[768,128]{1,0:T(8,128)(2,1)S(1)}, u32[]{:S(2)}, u32[]{:S(2)}) collective-permute-start(bf16[768,128]{1,0:T(8,128)(2,1)} %get-tuple-element.25), channel_id=1, source_target_pairs={{0,16},{1,20},{2,18},{3,22},{4,17},{5,21},{6,19},{7,23},{8,24},{9,... | collective-permute-start | bytes 589832 | tf_op jit(solution)/shard_map/ppermute | solution.py:297
  13.5 1.6 %collective-permute-start.1 = (bf16[768,128]{1,0:T(8,128)(2,1)}, bf16[768,128]{1,0:T(8,128)(2,1)S(1)}, u32[]{:S(2)}, u32[]{:S(2)}) collective-permute-start(bf16[768,128]{1,0:T(8,128)(2,1)} %get-tuple-element.23), channel_id=1, source_target_pairs={{0,0},{1,4},{2,2},{3,6},{4,1},{5,5},{6,3},{7,7},{8,8},{9,12},{10,1... | collective-permute-start | bytes 589832 | tf_op jit(solution)/shard_map/ppermute | solution.py:297
  15.1 1.6 %collective-permute-start = (bf16[768,128]{1,0:T(8,128)(2,1)}, bf16[768,128]{1,0:T(8,128)(2,1)S(1)}, u32[]{:S(2)}, u32[]{:S(2)}) collective-permute-start(bf16[768,128]{1,0:T(8,128)(2,1)} %get-tuple-element.22), channel_id=1, source_target_pairs={{0,8},{1,12},{2,10},{3,14},{4,9},{5,13},{6,11},{7,15},{8,0},{9,4},... | collective-permute-start | bytes 589832 | tf_op jit(solution)/shard_map/ppermute | solution.py:297
  16.7 6.4 %collective-permute-done.5.refs_2_.refs_0_ = bf16[768,128]{1,0:T(8,128)(2,1)S(1)} collective-permute-done((bf16[768,128]{1,0:T(8,128)(2,1)}, bf16[768,128]{1,0:T(8,128)(2,1)S(1)}, u32[]{:S(2)}, u32[]{:S(2)}) %collective-permute-start.5) | collective-permute-done | bytes 196640 | tf_op jit(solution)/shard_map/ppermute | solution.py:297
  23.2 2.2 %collective-permute-start.6 = (bf16[2,512,128]{2,1,0:T(8,128)(2,1)S(1)}, bf16[2,512,128]{2,1,0:T(8,128)(2,1)}, u32[]{:S(2)}, u32[]{:S(2)}) collective-permute-start(bf16[2,512,128]{2,1,0:T(8,128)(2,1)S(1)} %pad_maximum_fusion.2.refs_4_), channel_id=1, source_target_pairs={{0,2},{2,0},{4,6},{6,4},{8,10},{10,8},{12,14},{14,12},{16,18},{18,... | collective-permute-start | bytes 786440 | tf_op jit(solution)/shard_map/ppermute | solution.py:271
  25.4 3.6 %collective-permute-done.2.refs_3_.refs_1_ = bf16[768,128]{1,0:T(8,128)(2,1)S(1)} collective-permute-done((bf16[768,128]{1,0:T(8,128)(2,1)}, bf16[768,128]{1,0:T(8,128)(2,1)S(1)}, u32[]{:S(2)}, u32[]{:S(2)}) %collective-permute-start.2) | collective-permute-done | bytes 196640 | tf_op jit(solution)/shard_map/ppermute | solution.py:297
  29.1 1.6 %collective-permute-start.3 = (bf16[2,512,128]{2,1,0:T(8,128)(2,1)S(1)}, bf16[2,512,128]{2,1,0:T(8,128)(2,1)}, u32[]{:S(2)}, u32[]{:S(2)}) collective-permute-start(bf16[2,512,128]{2,1,0:T(8,128)(2,1)S(1)} %pad_maximum_fusion.1.refs_5_), channel_id=1, source_target_pairs={{0,2},{2,0},{4,6},{6,4},{8,10},{10,8},{12,14},{14,12},{16,18},{18,... | collective-permute-start | bytes 786440 | tf_op jit(solution)/shard_map/ppermute | solution.py:271
  30.6 0.6 collective-permute-start.16
  31.7 3.4 %collective-permute-done.10 = f32[4]{0:T(128)S(1)} collective-permute-done((f32[4]{0:T(128)S(1)}, f32[4]{0:T(128)S(1)}, u32[]{:S(2)}, u32[]{:S(2)}) %collective-permute-start.10) | collective-permute-done | bytes 48 | tf_op jit(solution)/shard_map/ppermute | solution.py:287
  35.6 2.7 %collective-permute-done.3.refs_2_ = bf16[2,512,128]{2,1,0:T(8,128)(2,1)} collective-permute-done((bf16[2,512,128]{2,1,0:T(8,128)(2,1)S(1)}, bf16[2,512,128]{2,1,0:T(8,128)(2,1)}, u32[]{:S(2)}, u32[]{:S(2)}) %collective-permute-start.3) | collective-permute-done | bytes 262176 | tf_op jit(solution)/shard_map/ppermute | solution.py:271
  38.3 0.8 copy.12.refs_8_
  39.0 0.6 dynamic_slice.3.refs_7_
  39.7 5.8 %attend.5 = (f32[4,8,512]{2,1,0:T(8,128)}, f32[4,8,512]{2,1,0:T(8,128)}, f32[4,128,512]{2,1,0:T(8,128)}) custom-call(bf16[768,128]{1,0:T(8,128)(2,1)} %copy-done, bf16[768,128]{1,0:T(8,128)(2,1)} %copy-done.1, bf16[768,128]{1,0:T(8,128)(2,1)} %copy-done.2, bf16[768,128]{1,0:T(8,128)(2,1)} %copy-done.3, bf16[2,512,128]{2,1,0:T(8,128)(2,1)} %copy-done.5, ...), custom_call_target="tpu_custom_call" | custom-call | tf_op jit(solution)/shard_map/attend/pallas_call | solution.py:196
  45.5 6.2 %attend.6 = (f32[4,8,512]{2,1,0:T(8,128)}, f32[4,8,512]{2,1,0:T(8,128)}, f32[4,128,512]{2,1,0:T(8,128)}) custom-call(bf16[768,128]{1,0:T(8,128)(2,1)} %copy-done, bf16[768,128]{1,0:T(8,128)(2,1)} %copy-done.1, bf16[768,128]{1,0:T(8,128)(2,1)} %copy-done.2, bf16[768,128]{1,0:T(8,128)(2,1)} %copy-done.3, bf16[2,512,128]{2,1,0:T(8,128)(2,1)} %collective-permute-done.8.refs_4_, ...), custom_call_target="tpu_custom_call" | custom-call | tf_op jit(solution)/shard_map/attend/pallas_call | solution.py:196
  51.7 6.2 %attend.7 = (f32[4,8,512]{2,1,0:T(8,128)}, f32[4,8,512]{2,1,0:T(8,128)}, f32[4,128,512]{2,1,0:T(8,128)}) custom-call(bf16[768,128]{1,0:T(8,128)(2,1)} %copy-done, bf16[768,128]{1,0:T(8,128)(2,1)} %copy-done.1, bf16[768,128]{1,0:T(8,128)(2,1)} %copy-done.2, bf16[768,128]{1,0:T(8,128)(2,1)} %copy-done.3, bf16[2,512,128]{2,1,0:T(8,128)(2,1)} %collective-permute-done.6.refs_4_, ...), custom_call_target="tpu_custom_call" | custom-call | tf_op jit(solution)/shard_map/attend/pallas_call | solution.py:196
  57.8 2.0 %concatenate.39.refs_6_ = f32[2,128,512]{2,1,0:T(8,128)} slice(f32[4,128,512]{2,1,0:T(8,128)} %get-tuple-element.34), slice={[2:4], [0:128], [0:512]} | slice | bytes 1048576 | tf_op jit(solution)/shard_map/concatenate | solution.py:323
  59.8 1.4 %concatenate.37.refs_4_ = f32[2,8,512]{2,1,0:T(8,128)} slice(f32[4,8,512]{2,1,0:T(8,128)} %get-tuple-element.32), slice={[2:4], [0:8], [0:512]} | slice | bytes 65536 | tf_op jit(solution)/shard_map/concatenate | solution.py:323
  61.2 1.4 %concatenate.38.refs_5_ = f32[2,8,512]{2,1,0:T(8,128)} slice(f32[4,8,512]{2,1,0:T(8,128)} %get-tuple-element.33), slice={[2:4], [0:8], [0:512]} | slice | bytes 65536 | tf_op jit(solution)/shard_map/concatenate | solution.py:323
  62.6 4.5 %attend.9 = (bf16[256,128]{1,0:T(8,128)(2,1)}, bf16[256,128]{1,0:T(8,128)(2,1)}) custom-call(bf16[768,128]{1,0:T(8,128)(2,1)} %copy-done.2, bf16[768,128]{1,0:T(8,128)(2,1)} %copy-done.3, bf16[2,512,128]{2,1,0:T(8,128)(2,1)} %collective-permute-done.3.refs_2_, bf16[2,512,128]{2,1,0:T(8,128)(2,1)} %collective-permute-done.4.refs_3_, ...), custom_call_target="tpu_custom_call" | custom-call | tf_op jit(solution)/shard_map/attend/pallas_call | solution.py:196
  67.0 4.6 %collective-permute-start.14 = (bf16[256,128]{1,0:T(8,128)(2,1)}, bf16[256,128]{1,0:T(8,128)(2,1)S(1)}, u32[]{:S(2)}, u32[]{:S(2)}) collective-permute-start(bf16[256,128]{1,0:T(8,128)(2,1)} %get-tuple-element.38), channel_id=1, source_target_pairs={{0,24},{1,28},{2,26},{3,30},{4,25},{5,29},{6,27},{7,31},{8,16},{9,... | collective-permute-start | bytes 196616 | tf_op jit(solution)/shard_map/ppermute | solution.py:297
  72.1 0.6 pad_maximum_fusion.7.refs_5_
  72.7 0.6 pad_maximum_fusion.6.refs_4_
  73.3 0.8 pad_maximum_fusion.refs_6_
  74.2 4.5 %attend.8 = (bf16[256,128]{1,0:T(8,128)(2,1)}, bf16[256,128]{1,0:T(8,128)(2,1)}) custom-call(bf16[768,128]{1,0:T(8,128)(2,1)} %copy-done.1, bf16[768,128]{1,0:T(8,128)(2,1)} %copy-done, bf16[2,512,128]{2,1,0:T(8,128)(2,1)} %collective-permute-done.3.refs_2_, bf16[2,512,128]{2,1,0:T(8,128)(2,1)} %collective-permute-done.4.refs_3_, ...), custom_call_target="tpu_custom_call" | custom-call | tf_op jit(solution)/shard_map/attend/pallas_call | solution.py:196
  78.6 1.5 %collective-permute-start.11 = (bf16[256,128]{1,0:T(8,128)(2,1)}, bf16[256,128]{1,0:T(8,128)(2,1)S(1)}, u32[]{:S(2)}, u32[]{:S(2)}) collective-permute-start(bf16[256,128]{1,0:T(8,128)(2,1)} %get-tuple-element.35), channel_id=1, source_target_pairs={{0,0},{1,4},{2,2},{3,6},{4,1},{5,5},{6,3},{7,7},{8,8},{9,12},{10,1... | collective-permute-start | bytes 196616 | tf_op jit(solution)/shard_map/ppermute | solution.py:297
  80.6 4.0 %collective-permute-done.12.refs_1_ = bf16[256,128]{1,0:T(8,128)(2,1)S(1)} collective-permute-done((bf16[256,128]{1,0:T(8,128)(2,1)}, bf16[256,128]{1,0:T(8,128)(2,1)S(1)}, u32[]{:S(2)}, u32[]{:S(2)}) %collective-permute-start.12) | collective-permute-done | bytes 65568 | tf_op jit(solution)/shard_map/ppermute | solution.py:297
  84.6 2.4 %collective-permute-start.15 = (bf16[4,256,128]{2,1,0:T(8,128)(2,1)S(1)}, bf16[4,256,128]{2,1,0:T(8,128)(2,1)S(1)}, u32[]{:S(2)}, u32[]{:S(2)}) collective-permute-start(bf16[4,256,128]{2,1,0:T(8,128)(2,1)S(1)} %pad_maximum_fusion.3), channel_id=1, source_target_pairs={{0,1},{1,0},{2,3},{3,2},{4,5},{5,4},{6,7},{7,6},{8,9},{9,8},{10,11... | collective-permute-start | bytes 786440 | tf_op jit(solution)/shard_map/ppermute | solution.py:350
  87.1 1.2 %collective-permute-done.15 = bf16[4,256,128]{2,1,0:T(8,128)(2,1)S(1)} collective-permute-done((bf16[4,256,128]{2,1,0:T(8,128)(2,1)S(1)}, bf16[4,256,128]{2,1,0:T(8,128)(2,1)S(1)}, u32[]{:S(2)}, u32[]{:S(2)}) %collective-permute-start.15) | collective-permute-done | bytes 262176 | tf_op jit(solution)/shard_map/ppermute | solution.py:350
  88.2 0.7 slice_bitcast_fusion.4
  89.0 5.0 %output.1 = bf16[256,2048]{1,0:T(8,128)(2,1)} custom-call(s32[1]{0:T(128)} %bitcast.zi, bf16[256,128]{1,0:T(8,128)(2,1)} %copy-done.10, bf16[256,128]{1,0:T(8,128)(2,1)} %copy-done.11, bf16[256,128]{1,0:T(8,128)(2,1)} %copy-done.9, bf16[256,128]{1,0:T(8,128)(2,1)} %copy-done.8, bf16[256,128]{1,0:T(8,128)(2,1)} %get-tuple-element.44.refs_4_, ...), custom_call_target="tpu_custom_call" | custom-call | tf_op jit(solution)/shard_map/output/pallas_call | solution.py:239
  (65 shorter events, 2.7 us)
Async XLA Ops:
  9.3 21.3 %copy-start.4 = (bf16[512,2048]{1,0:T(8,128)(2,1)S(1)}, bf16[512,2048]{1,0:T(8,128)(2,1)}, u32[]{:S(2)}) copy-start(bf16[512,2048]{1,0:T(8,128)(2,1)} %refs_8_.1) | copy-start | bytes 6291460
  9.3 21.8 %copy-start.15 = (f32[4]{0:T(128)S(1)}, f32[4]{0:T(128)}, u32[]{:S(2)}) copy-start(f32[4]{0:T(128)} %param.13) | copy-start | bytes 52
  9.3 28.9 %copy-start.14 = (f32[128]{0:T(128)S(1)}, f32[128]{0:T(128)}, u32[]{:S(2)}) copy-start(f32[128]{0:T(128)} %param.14) | copy-start | bytes 1540
  9.4 13.7 %collective-permute-start.5 = (bf16[768,128]{1,0:T(8,128)(2,1)}, bf16[768,128]{1,0:T(8,128)(2,1)S(1)}, u32[]{:S(2)}, u32[]{:S(2)}) collective-permute-start(bf16[768,128]{1,0:T(8,128)(2,1)} %get-tuple-element.25), channel_id=1, source_target_pairs={{0,16},{1,20},{2,18},{3,22},{4,17},{5,21},{6,19},{7,23},{8,24},{9,... | collective-permute-start | bytes 589832 | tf_op jit(solution)/shard_map/ppermute | solution.py:297
  13.5 9.6 %collective-permute-start.1 = (bf16[768,128]{1,0:T(8,128)(2,1)}, bf16[768,128]{1,0:T(8,128)(2,1)S(1)}, u32[]{:S(2)}, u32[]{:S(2)}) collective-permute-start(bf16[768,128]{1,0:T(8,128)(2,1)} %get-tuple-element.23), channel_id=1, source_target_pairs={{0,0},{1,4},{2,2},{3,6},{4,1},{5,5},{6,3},{7,7},{8,8},{9,12},{10,1... | collective-permute-start | bytes 589832 | tf_op jit(solution)/shard_map/ppermute | solution.py:297
  15.1 10.3 %collective-permute-start = (bf16[768,128]{1,0:T(8,128)(2,1)}, bf16[768,128]{1,0:T(8,128)(2,1)S(1)}, u32[]{:S(2)}, u32[]{:S(2)}) collective-permute-start(bf16[768,128]{1,0:T(8,128)(2,1)} %get-tuple-element.22), channel_id=1, source_target_pairs={{0,8},{1,12},{2,10},{3,14},{4,9},{5,13},{6,11},{7,15},{8,0},{9,4},... | collective-permute-start | bytes 589832 | tf_op jit(solution)/shard_map/ppermute | solution.py:297
  16.6 12.3 %collective-permute-start.2 = (bf16[768,128]{1,0:T(8,128)(2,1)}, bf16[768,128]{1,0:T(8,128)(2,1)S(1)}, u32[]{:S(2)}, u32[]{:S(2)}) collective-permute-start(bf16[768,128]{1,0:T(8,128)(2,1)} %get-tuple-element.24), channel_id=1, source_target_pairs={{0,24},{1,28},{2,26},{3,30},{4,25},{5,29},{6,27},{7,31},{8,16},{9,... | collective-permute-start | bytes 589832 | tf_op jit(solution)/shard_map/ppermute | solution.py:297
  23.1 16.6 %copy-start.2 = (bf16[768,128]{1,0:T(8,128)(2,1)}, bf16[768,128]{1,0:T(8,128)(2,1)S(1)}, u32[]{:S(2)}) copy-start(bf16[768,128]{1,0:T(8,128)(2,1)S(1)} %collective-permute-done.5.refs_2_.refs_0_) | copy-start | bytes 589828
  23.1 16.5 %copy-start = (bf16[768,128]{1,0:T(8,128)(2,1)}, bf16[768,128]{1,0:T(8,128)(2,1)S(1)}, u32[]{:S(2)}) copy-start(bf16[768,128]{1,0:T(8,128)(2,1)S(1)} %collective-permute-done.1.refs_0_.refs_1_) | copy-start | bytes 589828
  23.1 16.5 %copy-start.5 = (bf16[2,512,128]{2,1,0:T(8,128)(2,1)}, bf16[2,512,128]{2,1,0:T(8,128)(2,1)S(1)}, u32[]{:S(2)}) copy-start(bf16[2,512,128]{2,1,0:T(8,128)(2,1)S(1)} %pad_maximum_fusion.2.refs_4_) | copy-start | bytes 786436
  23.2 12.3 %collective-permute-start.6 = (bf16[2,512,128]{2,1,0:T(8,128)(2,1)S(1)}, bf16[2,512,128]{2,1,0:T(8,128)(2,1)}, u32[]{:S(2)}, u32[]{:S(2)}) collective-permute-start(bf16[2,512,128]{2,1,0:T(8,128)(2,1)S(1)} %pad_maximum_fusion.2.refs_4_), channel_id=1, source_target_pairs={{0,2},{2,0},{4,6},{6,4},{8,10},{10,8},{12,14},{14,12},{16,18},{18,... | collective-permute-start | bytes 786440 | tf_op jit(solution)/shard_map/ppermute | solution.py:271
  25.4 14.3 %copy-start.1 = (bf16[768,128]{1,0:T(8,128)(2,1)}, bf16[768,128]{1,0:T(8,128)(2,1)S(1)}, u32[]{:S(2)}) copy-start(bf16[768,128]{1,0:T(8,128)(2,1)S(1)} %collective-permute-done.refs_1_.refs_0_) | copy-start | bytes 589828
  29.0 10.6 %copy-start.3 = (bf16[768,128]{1,0:T(8,128)(2,1)}, bf16[768,128]{1,0:T(8,128)(2,1)S(1)}, u32[]{:S(2)}) copy-start(bf16[768,128]{1,0:T(8,128)(2,1)S(1)} %collective-permute-done.2.refs_3_.refs_1_) | copy-start | bytes 589828
  29.0 10.6 %copy-start.6 = (bf16[2,512,128]{2,1,0:T(8,128)(2,1)}, bf16[2,512,128]{2,1,0:T(8,128)(2,1)S(1)}, u32[]{:S(2)}) copy-start(bf16[2,512,128]{2,1,0:T(8,128)(2,1)S(1)} %pad_maximum_fusion.1.refs_5_) | copy-start | bytes 786436
  29.1 9.2 %collective-permute-start.3 = (bf16[2,512,128]{2,1,0:T(8,128)(2,1)S(1)}, bf16[2,512,128]{2,1,0:T(8,128)(2,1)}, u32[]{:S(2)}, u32[]{:S(2)}) collective-permute-start(bf16[2,512,128]{2,1,0:T(8,128)(2,1)S(1)} %pad_maximum_fusion.1.refs_5_), channel_id=1, source_target_pairs={{0,2},{2,0},{4,6},{6,4},{8,10},{10,8},{12,14},{14,12},{16,18},{18,... | collective-permute-start | bytes 786440 | tf_op jit(solution)/shard_map/ppermute | solution.py:271
  30.6 58.4 %collective-permute-start.16 = (bf16[512,2048]{1,0:T(8,128)(2,1)S(1)}, bf16[512,2048]{1,0:T(8,128)(2,1)}, u32[]{:S(2)}, u32[]{:S(2)}) collective-permute-start(bf16[512,2048]{1,0:T(8,128)(2,1)S(1)} %copy-done.4), channel_id=1, source_target_pairs={{0,1},{1,0},{2,3},{3,2},{4,5},{5,4},{6,7},{7,6},{8,9},{9,8},{10,11... | collective-permute-start | bytes 6291464 | tf_op jit(solution)/shard_map/ppermute | solution.py:349
  31.2 3.9 %collective-permute-start.10 = (f32[4]{0:T(128)S(1)}, f32[4]{0:T(128)S(1)}, u32[]{:S(2)}, u32[]{:S(2)}) collective-permute-start(f32[4]{0:T(128)S(1)} %copy-done.15), channel_id=1, source_target_pairs={{0,1},{1,0},{2,3},{3,2},{4,5},{5,4},{6,7},{7,6},{8,9},{9,8},{10,11... | collective-permute-start | bytes 56 | tf_op jit(solution)/shard_map/ppermute | solution.py:287
  31.2 14.2 %collective-permute-start.8 = (bf16[2,512,128]{2,1,0:T(8,128)(2,1)S(1)}, bf16[2,512,128]{2,1,0:T(8,128)(2,1)}, u32[]{:S(2)}, u32[]{:S(2)}) collective-permute-start(bf16[2,512,128]{2,1,0:T(8,128)(2,1)S(1)} %pad_maximum_fusion.2.refs_4_), channel_id=1, source_target_pairs={{0,1},{1,0},{2,3},{3,2},{4,5},{5,4},{6,7},{7,6},{8,9},{9,8},{10,11... | collective-permute-start | bytes 786440 | tf_op jit(solution)/shard_map/ppermute | solution.py:309
  35.1 10.4 %collective-permute-start.9 = (bf16[2,512,128]{2,1,0:T(8,128)(2,1)S(1)}, bf16[2,512,128]{2,1,0:T(8,128)(2,1)}, u32[]{:S(2)}, u32[]{:S(2)}) collective-permute-start(bf16[2,512,128]{2,1,0:T(8,128)(2,1)S(1)} %pad_maximum_fusion.1.refs_5_), channel_id=1, source_target_pairs={{0,1},{1,0},{2,3},{3,2},{4,5},{5,4},{6,7},{7,6},{8,9},{9,8},{10,11... | collective-permute-start | bytes 786440 | tf_op jit(solution)/shard_map/ppermute | solution.py:309
  35.5 16.2 %collective-permute-start.7 = (bf16[2,512,128]{2,1,0:T(8,128)(2,1)}, bf16[2,512,128]{2,1,0:T(8,128)(2,1)}, u32[]{:S(2)}, u32[]{:S(2)}) collective-permute-start(bf16[2,512,128]{2,1,0:T(8,128)(2,1)} %collective-permute-done.6.refs_4_), channel_id=1, source_target_pairs={{0,1},{1,0},{2,3},{3,2},{4,5},{5,4},{6,7},{7,6},{8,9},{9,8},{10,11... | collective-permute-start | bytes 786440 | tf_op jit(solution)/shard_map/ppermute | solution.py:309
  38.3 24.3 %collective-permute-start.4 = (bf16[2,512,128]{2,1,0:T(8,128)(2,1)}, bf16[2,512,128]{2,1,0:T(8,128)(2,1)}, u32[]{:S(2)}, u32[]{:S(2)}) collective-permute-start(bf16[2,512,128]{2,1,0:T(8,128)(2,1)} %collective-permute-done.3.refs_2_), channel_id=1, source_target_pairs={{0,1},{1,0},{2,3},{3,2},{4,5},{5,4},{6,7},{7,6},{8,9},{9,8},{10,11... | collective-permute-start | bytes 786440 | tf_op jit(solution)/shard_map/ppermute | solution.py:309
  57.8 14.2 %copy-start.13 = (f32[4,8,512]{2,1,0:T(8,128)S(1)}, f32[4,8,512]{2,1,0:T(8,128)}, u32[]{:S(2)}) copy-start(f32[4,8,512]{2,1,0:T(8,128)} %get-tuple-element.33) | copy-start | bytes 196612
  57.8 14.8 %copy-start.12 = (f32[4,8,512]{2,1,0:T(8,128)S(1)}, f32[4,8,512]{2,1,0:T(8,128)}, u32[]{:S(2)}) copy-start(f32[4,8,512]{2,1,0:T(8,128)} %get-tuple-element.32) | copy-start | bytes 196612
  57.8 15.4 %copy-start.7 = (f32[4,128,512]{2,1,0:T(8,128)S(1)}, f32[4,128,512]{2,1,0:T(8,128)}, u32[]{:S(2)}) copy-start(f32[4,128,512]{2,1,0:T(8,128)} %get-tuple-element.34) | copy-start | bytes 3145732
  67.0 13.5 %collective-permute-start.14 = (bf16[256,128]{1,0:T(8,128)(2,1)}, bf16[256,128]{1,0:T(8,128)(2,1)S(1)}, u32[]{:S(2)}, u32[]{:S(2)}) collective-permute-start(bf16[256,128]{1,0:T(8,128)(2,1)} %get-tuple-element.38), channel_id=1, source_target_pairs={{0,24},{1,28},{2,26},{3,30},{4,25},{5,29},{6,27},{7,31},{8,16},{9,... | collective-permute-start | bytes 196616 | tf_op jit(solution)/shard_map/ppermute | solution.py:297
  71.6 9.0 %collective-permute-start.13 = (bf16[256,128]{1,0:T(8,128)(2,1)}, bf16[256,128]{1,0:T(8,128)(2,1)S(1)}, u32[]{:S(2)}, u32[]{:S(2)}) collective-permute-start(bf16[256,128]{1,0:T(8,128)(2,1)} %get-tuple-element.37), channel_id=1, source_target_pairs={{0,16},{1,20},{2,18},{3,22},{4,17},{5,21},{6,19},{7,23},{8,24},{9,... | collective-permute-start | bytes 196616 | tf_op jit(solution)/shard_map/ppermute | solution.py:297
  78.6 1.9 %collective-permute-start.11 = (bf16[256,128]{1,0:T(8,128)(2,1)}, bf16[256,128]{1,0:T(8,128)(2,1)S(1)}, u32[]{:S(2)}, u32[]{:S(2)}) collective-permute-start(bf16[256,128]{1,0:T(8,128)(2,1)} %get-tuple-element.35), channel_id=1, source_target_pairs={{0,0},{1,4},{2,2},{3,6},{4,1},{5,5},{6,3},{7,7},{8,8},{9,12},{10,1... | collective-permute-start | bytes 196616 | tf_op jit(solution)/shard_map/ppermute | solution.py:297
  80.1 4.5 %collective-permute-start.12 = (bf16[256,128]{1,0:T(8,128)(2,1)}, bf16[256,128]{1,0:T(8,128)(2,1)S(1)}, u32[]{:S(2)}, u32[]{:S(2)}) collective-permute-start(bf16[256,128]{1,0:T(8,128)(2,1)} %get-tuple-element.36), channel_id=1, source_target_pairs={{0,8},{1,12},{2,10},{3,14},{4,9},{5,13},{6,11},{7,15},{8,0},{9,4},... | collective-permute-start | bytes 196616 | tf_op jit(solution)/shard_map/ppermute | solution.py:297
  80.6 8.4 %copy-start.8 = (bf16[256,128]{1,0:T(8,128)(2,1)}, bf16[256,128]{1,0:T(8,128)(2,1)S(1)}, u32[]{:S(2)}) copy-start(bf16[256,128]{1,0:T(8,128)(2,1)S(1)} %collective-permute-done.14.refs_3_) | copy-start | bytes 196612
  80.6 8.4 %copy-start.9 = (bf16[256,128]{1,0:T(8,128)(2,1)}, bf16[256,128]{1,0:T(8,128)(2,1)S(1)}, u32[]{:S(2)}) copy-start(bf16[256,128]{1,0:T(8,128)(2,1)S(1)} %collective-permute-done.13.refs_2_) | copy-start | bytes 196612
  80.6 8.4 %copy-start.10 = (bf16[256,128]{1,0:T(8,128)(2,1)}, bf16[256,128]{1,0:T(8,128)(2,1)S(1)}, u32[]{:S(2)}) copy-start(bf16[256,128]{1,0:T(8,128)(2,1)S(1)} %collective-permute-done.11.refs_0_) | copy-start | bytes 196612
  84.6 3.6 %collective-permute-start.15 = (bf16[4,256,128]{2,1,0:T(8,128)(2,1)S(1)}, bf16[4,256,128]{2,1,0:T(8,128)(2,1)S(1)}, u32[]{:S(2)}, u32[]{:S(2)}) collective-permute-start(bf16[4,256,128]{2,1,0:T(8,128)(2,1)S(1)} %pad_maximum_fusion.3), channel_id=1, source_target_pairs={{0,1},{1,0},{2,3},{3,2},{4,5},{5,4},{6,7},{7,6},{8,9},{9,8},{10,11... | collective-permute-start | bytes 786440 | tf_op jit(solution)/shard_map/ppermute | solution.py:350
  (1 other events, 4.4 us)
